TPU v7x, 1024 devices: a whole 4x4x32 slice. The times are simulated.
1024 devices in a mesh: sp: 32 (over z), tp: 4 (over y), dp: 8 (over x, core).
Axes of the slice: x: 4, y: 4, z: 32, core: 2. Of those that a mesh axis runs over, the one named last changes fastest.
Arguments:
- latent: bfloat16 [32768, 2048], P(('dp', 'sp', 'tp')), parts along dimension 0, may hold values from -6 to 6
- cond: bfloat16 [16384], P('dp'), parts along dimension 0, may hold values from -6 to 6
- context: bfloat16 [4096, 2048], P(('dp', 'sp')), parts along dimension 0, may hold values from -6 to 6
- context_cond: bfloat16 [2048], replicated, may hold values from -6 to 6
- modulation: bfloat16 [2048, 6144], P(('sp', 'tp')), may hold values from -0.125 to 0.125
- norm_gain: bfloat16 [2048], replicated, may hold values from 0.099609375 to 1.8984375
- w_x: bfloat16 [2048, 1024], P(None, 'tp'), may hold values from -0.125 to 0.125
- w_gate: bfloat16 [2048, 1024], P(None, 'tp'), may hold values from -0.125 to 0.125
- w_b: bfloat16 [2048, 256], P(None, 'tp'), may hold values from -0.125 to 0.125
- w_c: bfloat16 [2048, 256], P(None, 'tp'), may hold values from -0.125 to 0.125
- w_dt: bfloat16 [2, 2048, 16], P(None, None, 'tp'), may hold values from -0.125 to 0.125
- conv_x: bfloat16 [4, 1024], P(None, 'tp'), may hold values from -3 to 3
- conv_b: bfloat16 [4, 256], P(None, 'tp'), may hold values from -3 to 3
- conv_c: bfloat16 [4, 256], P(None, 'tp'), may hold values from -3 to 3
- decay_rate: float32 [2, 16], P(None, 'tp'), may hold values from 0 to 0.04
- decay_extra: float32 [32768, 16], P(('dp', 'sp'), 'tp'), parts along dimension 0, may hold values from -2 to 0
- out_gain: bfloat16 [1024], P('tp'), may hold values from 0.099609375 to 1.8984375
- w_out: bfloat16 [1024, 2048], replicated, may hold values from -0.1875 to 0.1875
Outputs:
- mixed: bfloat16 [32768, 2048], P(('dp', 'sp', 'tp')), parts along dimension 0
There are 8 independent parts, one for each index of `dp`. A program takes and returns all parts, laid end to end along the dimension named above; an argument that names none is the same for every part. Nothing has to cross between parts.
All inputs are finite; a program needn't handle non-finite values.
Results may differ from a plain program's by a relative error of at most 0.007.
Values may be sent and summed in bfloat16 or wider, within the bound.
No kernel may reach another device: no remote copies, remote signals or barrier semaphores. Data moves between devices by JAX's collectives and lax.ppermute only.
A program may use at most 64 MiB of HBM per device.

v0:
```python
import functools

import jax
import jax.numpy as jnp
from jax import lax
from jax.sharding import PartitionSpec as P

HEAD_DIM = 64
STATE = 64
BLOCK = 128


ROW_EPS = 1e-06
GROUP_EPS = 1e-05
HIGHEST = lax.Precision.HIGHEST


def prefix(x, axis, join, neutral, backward):
    count = lax.axis_size(axis)
    place = lax.axis_index(axis)
    ahead = count - 1 - place if backward else place
    gathered = jax.tree.map(
        lambda a, kind: lax.all_gather(a.astype(kind), axis),
        x,
        jax.tree.map(lambda a: jnp.bfloat16 if a.dtype == jnp.float32 else a.dtype, x),
    )
    state = jax.tree.map(lambda a, e: jnp.zeros_like(a) + jnp.asarray(e, a.dtype), x, neutral)

    def one(hop, state):
        source = count - 1 - hop if backward else hop
        return join(
            state,
            jax.tree.map(
                lambda a, own: lax.dynamic_index_in_dim(a, source, 0, False).astype(own.dtype),
                gathered,
                x,
            ),
        )

    return lax.fori_loop(0, ahead, one, state)


def over_axes(x, axes):
    return functools.reduce(lax.psum, axes, x)


def from_everyone(x, axis):
    length = lax.axis_size(axis)
    return lax.all_to_all(jnp.broadcast_to(x[None], (length, *x.shape)), axis, 0, 0, tiled=True)


def in_order(blocks, dim):
    blocks = jnp.moveaxis(blocks, 0, dim)
    shape = blocks.shape
    return blocks.reshape(*shape[:dim], shape[dim] * shape[dim + 1], *shape[dim + 2 :])


def gathered_copies(x, axis, dim):
    blocks = from_everyone(x, axis)
    return in_order(blocks, dim)


def with_halo(block, sides, width):
    for axis, dim in sides:
        count = lax.axis_size(axis)
        forward = [(i, i + 1) for i in range(count - 1)]
        backward = [(target, source) for source, target in forward]
        low = lax.ppermute(
            lax.slice_in_dim(block, block.shape[dim] - width, None, axis=dim), axis, forward
        )
        high = lax.ppermute(lax.slice_in_dim(block, 0, width, axis=dim), axis, backward)
        block = jnp.concatenate([low, block, high], axis=dim)
    return block


def modulated_norm(row_block, norm_gain, shift_row, scale_row):
    values = row_block.astype(jnp.float32)
    normed = values * lax.rsqrt(jnp.mean(values * values, axis=-1, keepdims=True) + ROW_EPS)
    return (normed * norm_gain.astype(jnp.float32) * (1.0 + scale_row) + shift_row).astype(
        jnp.bfloat16
    )


def project_many(row_block, weights):
    return jnp.concatenate(
        [
            jnp.dot(row_block, weight, preferred_element_type=jnp.float32).astype(jnp.bfloat16)
            for weight in weights
        ],
        axis=1,
    )


def conv_padded(padded, conv_taps, length):
    values = padded.astype(jnp.float32)
    summed = jnp.zeros((length, values.shape[1]), jnp.float32)
    for offset in range(conv_taps.shape[0]):
        summed = summed + conv_taps[offset].astype(jnp.float32) * values[offset : offset + length]
    return jax.nn.silu(summed).astype(jnp.bfloat16)


def context_states(ctx_xs, ctx_bmat, ctx_dt, decay_rate):
    length = ctx_xs.shape[0]
    groups = ctx_bmat.shape[1] // STATE
    heads_here = ctx_dt.shape[2]
    repeat = heads_here // groups
    values = ctx_xs.astype(jnp.float32).reshape(length, groups, repeat, HEAD_DIM)
    keys_b = ctx_bmat.astype(jnp.float32).reshape(length, groups, STATE)
    log_decay = -decay_rate[:, None, :] * ctx_dt
    running = jnp.cumsum(log_decay, axis=1)
    forward_weight = (jnp.exp(running[0, -1:] - running[0]) * ctx_dt[0]).reshape(
        length, groups, repeat
    )
    backward_weight = (jnp.exp(running[1] - log_decay[1]) * ctx_dt[1]).reshape(
        length, groups, repeat
    )
    forward_state = jnp.einsum(
        "lgn,lgr,lgrp->grpn", keys_b, forward_weight, values, precision=HIGHEST
    )
    backward_state = jnp.einsum(
        "lgn,lgr,lgrp->grpn", keys_b, backward_weight, values, precision=HIGHEST
    )
    return (forward_state, backward_state)


def block_pass(inputs, step_sizes, log_decay, bmat, cmat, start_state):
    length = inputs.shape[0]
    groups, repeat = (start_state.shape[0], start_state.shape[1])
    block_count = length // BLOCK
    values = inputs.reshape(block_count, BLOCK, groups, repeat, HEAD_DIM)
    steps_blk = step_sizes.reshape(block_count, BLOCK, groups, repeat)
    decays = log_decay.reshape(block_count, BLOCK, groups, repeat)
    keys_b = bmat.reshape(block_count, BLOCK, groups, STATE)
    reads_c = cmat.reshape(block_count, BLOCK, groups, STATE)
    lower_mask = (jnp.arange(BLOCK)[:, None] >= jnp.arange(BLOCK)[None, :])[:, :, None, None]

    def advance(carried, block_data):
        value_blk, step_blk, decay_blk, key_blk, read_blk = block_data
        running = jnp.cumsum(decay_blk, axis=0)
        log_gaps = running[:, None] - running[None, :]
        mixing = jnp.where(lower_mask, jnp.exp(jnp.where(lower_mask, log_gaps, 0.0)), 0.0)
        affinity = jnp.einsum("ign,jgn->ijg", read_blk, key_blk, preferred_element_type=jnp.float32)
        weights = (affinity[..., None] * mixing * step_blk[None]).astype(jnp.bfloat16)
        output = jnp.einsum(
            "ijgr,jgrp->igrp", weights, value_blk, preferred_element_type=jnp.float32
        )
        output = output + jnp.einsum(
            "ign,grpn,igr->igrp",
            read_blk.astype(jnp.float32),
            carried,
            jnp.exp(running),
            precision=HIGHEST,
        )
        to_end = jnp.exp(running[-1:] - running) * step_blk
        state_in = (key_blk.astype(jnp.float32)[:, :, None, :] * to_end[..., None]).astype(
            jnp.bfloat16
        )
        carried = jnp.exp(running[-1])[..., None, None] * carried + jnp.einsum(
            "jgrn,jgrp->grpn", state_in, value_blk, preferred_element_type=jnp.float32
        )
        return (carried, output)

    final_state, outputs = lax.scan(
        advance, start_state, (values, steps_blk, decays, keys_b, reads_c)
    )
    return (outputs.reshape(length, groups, repeat, HEAD_DIM), final_state)


def state_chain(summary, backward):

    def combine(earlier, later_part):
        return (
            earlier[0] + later_part[0],
            jnp.exp(later_part[0])[..., None, None] * earlier[1] + later_part[1],
        )

    identity_pair = (jnp.zeros_like(summary[0]), jnp.zeros_like(summary[1]))
    return prefix(summary, "sp", combine, identity_pair, backward)


def directed_pass(inputs, step_sizes, log_decay, bmat, cmat, outer_start, zeros_state, backward):
    local_out, final_state = block_pass(inputs, step_sizes, log_decay, bmat, cmat, zeros_state)
    length = inputs.shape[0]
    groups, repeat = (zeros_state.shape[0], zeros_state.shape[1])
    running = jnp.cumsum(log_decay, axis=0).reshape(length, groups, repeat)
    before = state_chain((running[-1], final_state), backward)
    entry_state = jnp.exp(before[0])[..., None, None] * outer_start + before[1]
    read_rows = cmat.astype(jnp.float32).reshape(length, groups, STATE)
    return local_out + jnp.einsum(
        "tgn,grpn,tgr->tgrp", read_rows, entry_state, jnp.exp(running), precision=HIGHEST
    )


def group_norm(combined, out_gain):
    length, groups, repeat, _ = combined.shape
    mean_square = jnp.mean(combined * combined, axis=(2, 3), keepdims=True)
    scaled = (
        combined
        * lax.rsqrt(mean_square + GROUP_EPS)
        * out_gain.astype(jnp.float32).reshape(groups, repeat, HEAD_DIM)
    )
    return scaled.reshape(length, groups * repeat * HEAD_DIM).astype(jnp.bfloat16)


def local(
    latent,
    cond,
    context,
    context_cond,
    modulation,
    norm_gain,
    w_x,
    w_gate,
    w_b,
    w_c,
    w_dt,
    conv_x,
    conv_b,
    conv_c,
    decay_rate,
    decay_extra,
    out_gain,
    w_out,
):
    model_width = latent.shape[1]
    mod_share = modulation.shape[0]
    cond_rows = jax.nn.silu(jnp.stack([cond, context_cond]).astype(jnp.float32)).astype(
        jnp.bfloat16
    )
    own_cols = lax.dynamic_slice_in_dim(
        cond_rows, lax.axis_index(("sp", "tp")) * mod_share, mod_share, 1
    )
    mod_rows = over_axes(
        jnp.dot(own_cols, modulation, preferred_element_type=jnp.float32), ("sp", "tp")
    )
    shift_rows = mod_rows[:, :model_width]
    scale_rows = mod_rows[:, model_width : 2 * model_width]
    gate_row = mod_rows[0, 2 * model_width :]
    head_cols = w_x.shape[1]
    state_cols = w_b.shape[1]
    heads_here = w_dt.shape[2]
    groups_here = state_cols // STATE
    repeat = heads_here // groups_here
    hidden = modulated_norm(latent, norm_gain, shift_rows[0], scale_rows[0])
    latent_mats = (w_x, w_b, w_c, w_gate, w_dt[0], w_dt[1])
    projected = project_many(gathered_copies(hidden, "tp", 0), latent_mats)
    token_count = projected.shape[0]
    conv_cols = head_cols + 2 * state_cols
    extended = with_halo(projected[:, :conv_cols], (("sp", 0),), 2)
    conv_taps = jnp.concatenate([conv_x, conv_b, conv_c], axis=1)
    convolved = conv_padded(extended, conv_taps, token_count)
    latent_xs = convolved[:, :head_cols]
    latent_b = convolved[:, head_cols : head_cols + state_cols]
    latent_c = convolved[:, head_cols + state_cols :]
    gate_in = projected[:, conv_cols : conv_cols + head_cols]
    dt_start = conv_cols + head_cols
    latent_dt = jnp.stack(
        [
            jax.nn.softplus(projected[:, dt_start : dt_start + heads_here].astype(jnp.float32)),
            jax.nn.softplus(projected[:, dt_start + heads_here :].astype(jnp.float32)),
        ]
    )
    context_mats = (w_x, w_b, w_dt[0], w_dt[1])
    own_context = project_many(
        modulated_norm(context, norm_gain, shift_rows[1], scale_rows[1]), context_mats
    )
    context_cols = gathered_copies(own_context, "sp", 0)
    ctx_span = head_cols + state_cols
    ctx_padded = jnp.pad(context_cols[:, :ctx_span], ((2, 1), (0, 0)))
    ctx_conv = conv_padded(
        ctx_padded, jnp.concatenate([conv_x, conv_b], axis=1), context_cols.shape[0]
    )
    ctx_dt = jnp.stack(
        [
            jax.nn.softplus(context_cols[:, ctx_span : ctx_span + heads_here].astype(jnp.float32)),
            jax.nn.softplus(context_cols[:, ctx_span + heads_here :].astype(jnp.float32)),
        ]
    )
    forward_start, backward_start = context_states(
        ctx_conv[:, :head_cols], ctx_conv[:, head_cols:], ctx_dt, decay_rate
    )
    log_decay = -decay_rate[:, None, :] * latent_dt + decay_extra[None]
    zeros_state = jnp.zeros((groups_here, repeat, HEAD_DIM, STATE), jnp.float32)
    y_forward = directed_pass(
        latent_xs, latent_dt[0], log_decay[0], latent_b, latent_c, forward_start, zeros_state, False
    )
    y_backward = directed_pass(
        latent_xs[::-1],
        latent_dt[1][::-1],
        log_decay[1][::-1],
        latent_b[::-1],
        latent_c[::-1],
        backward_start,
        zeros_state,
        True,
    )
    gate_act = jax.nn.silu(gate_in.astype(jnp.float32)).reshape(
        token_count, groups_here, repeat, HEAD_DIM
    )
    combined = (y_forward + y_backward[::-1]) * gate_act
    normed = group_norm(combined, out_gain)
    tp_count = lax.axis_size("tp")
    stacked = normed.reshape(tp_count, token_count // tp_count, normed.shape[1])
    branch = jnp.dot(
        lax.all_to_all(stacked, "tp", split_axis=0, concat_axis=2, tiled=True)[0],
        w_out,
        preferred_element_type=jnp.float32,
    )[None]
    return (latent.astype(jnp.float32) + gate_row * branch[0]).astype(jnp.bfloat16)


def solution(mesh):
    in_specs = (
        P(("dp", "sp", "tp"), None),
        P("dp"),
        P(("dp", "sp"), None),
        P(),
        P(("sp", "tp"), None),
        P(),
        P(None, "tp"),
        P(None, "tp"),
        P(None, "tp"),
        P(None, "tp"),
        P(None, None, "tp"),
        P(None, "tp"),
        P(None, "tp"),
        P(None, "tp"),
        P(None, "tp"),
        P(("dp", "sp"), "tp"),
        P("tp"),
        P(),
    )
    out_specs = P(("dp", "sp", "tp"), None)
    return jax.shard_map(local, mesh=mesh, in_specs=in_specs, out_specs=out_specs, check_vma=False)
```

profile of v0, /device:TPU:2, one launch (start us, length us, event | category | flops | bytes accessed | tf_op | source)
XLA Modules:
  0.0 525.9 jit_solution(17267531133946643762)
XLA Ops:
  6.6 1.1 fusion.28
  9.8 1.2 fusion.103
  11.0 120.7 %psum.14 = f32[2,6144]{1,0:T(2,128)S(1)} all-reduce(f32[2,6144]{1,0:T(2,128)S(1)} %fusion.103), channel_id=1, replica_groups=mesh['sp'=32,'tp'=4,'dp'=8] {'sp'}, use_global_device_ids=true, to_apply=%region_0.1 | all-reduce | flops 12288 | bytes 98304 | tf_op jit(solution)/shard_map/psum | solution.py:44
  131.7 17.6 %psum.15 = f32[2,6144]{1,0:T(2,128)S(1)} all-reduce(f32[2,6144]{1,0:T(2,128)S(1)} %psum.14), channel_id=1, replica_groups=mesh['sp'=32,'tp'=4,'dp'=8] {'tp'}, use_global_device_ids=true, to_apply=%region_1.2 | all-reduce | flops 12288 | bytes 98304 | tf_op jit(solution)/shard_map/psum | solution.py:44
  149.4 1.0 fusion.32
  151.2 3.5 all-to-all-start
  154.7 1.0 fusion.38
  155.7 0.9 fusion.42
  159.2 1.1 convolution_convert_fusion.5
  161.0 1.8 all-to-all-done
  163.6 13.0 %all-to-all-start.1 = ((bf16[32,16,328]{2,1,0:T(8,128)(2,1)}), bf16[32,16,328]{2,1,0:T(8,128)(2,1)S(1)}, u32[]{:S(2)}, u32[]{:S(2)}) async-start(bf16[32,16,328]{2,1,0:T(8,128)(2,1)} %broadcast_in_dim.112), calls=%async_computation.1 | async-start | bytes 786432 | tf_op jit(solution)/shard_map/all_to_all | solution.py:49
  178.8 1.6 divide_multiply_fusion
  180.4 3.7 collective-permute-start
  184.2 1.3 collective-permute-start.1
  185.7 6.5 %collective-permute-done = bf16[2,384]{0,1:T(8,128)(2,1)S(1)} collective-permute-done((bf16[2,384]{0,1:T(8,128)(2,1)S(1)}, bf16[2,384]{0,1:T(8,128)(2,1)S(1)}, u32[]{:S(2)}, u32[]{:S(2)}) %collective-permute-start) | collective-permute-done | bytes 1568 | tf_op jit(solution)/shard_map/ppermute | solution.py:68
  192.2 3.0 collective-permute-done.1
  197.9 58.1 %all-gather.4 = bf16[32,1,4]{2,1,0:T(2,128)(2,1)S(1)} all-gather(bf16[1,1,4]{2,1,0:T(2,128)(2,1)S(1)} %fusion.106), channel_id=2, replica_groups=mesh['sp'=32,'tp'=4,'dp'=8] {'sp'}, dimensions={0}, use_global_device_ids=true | all-gather | bytes 264 | tf_op jit(solution)/shard_map/all_gather | solution.py:23
  256.0 53.0 %all-gather.5 = bf16[32,1,4]{2,1,0:T(2,128)(2,1)S(1)} all-gather(bf16[1,1,4]{2,1,0:T(2,128)(2,1)S(1)} %fusion.105), channel_id=4, replica_groups=mesh['sp'=32,'tp'=4,'dp'=8] {'sp'}, dimensions={0}, use_global_device_ids=true | all-gather | bytes 264 | tf_op jit(solution)/shard_map/all_gather | solution.py:23
  311.8 24.1 %all-gather.9.cloned.1.call-done = bf16[128,64,64]{2,1,0:T(8,128)(2,1)} async-done(((bf16[4,64,64]{2,1,0:T(8,128)(2,1)}), bf16[128,64,64]{2,1,0:T(8,128)(2,1)}) %all-gather.9.cloned.1.call-update) | async-done | bytes 1048592 | tf_op jit(solution)/shard_map/all_gather | solution.py:23
  336.0 131.9 %all-gather.11.cloned.1.call-done = bf16[128,64,64]{2,1,0:T(8,128)(2,1)} async-done(((bf16[4,64,64]{2,1,0:T(8,128)(2,1)}), bf16[128,64,64]{2,1,0:T(8,128)(2,1)}) %all-gather.11.cloned.1.call-update) | async-done | bytes 1048592 | tf_op jit(solution)/shard_map/all_gather | solution.py:23
  468.0 30.7 %while.7 = (s32[]{:T(128)}, f32[1,4]{1,0:T(1,128)S(1)}, f32[1,4,64,64]{3,2,1,0:T(8,128)S(1)}, s32[]{:T(128)}, bf16[32,1,4]{2,1,0:T(2,128)(2,1)S(1)}, /*index=5*/...) while((s32[]{:T(128)}, f32[1,4]{1,0:T(1,128)S(1)}, ...), condition=%wide.region_13.14_spmd, body=%wide.region_12.13_spmd.sunk | while | flops 49170 | bytes 164087 | solution.py:40
  468.1 0.9 convert_add_fusion.5
  469.1 0.9 convert_add_fusion.5
  470.0 0.9 convert_add_fusion.5
  471.0 0.9 convert_add_fusion.5
  472.0 0.9 convert_add_fusion.5
  473.0 0.9 convert_add_fusion.5
  474.0 0.9 convert_add_fusion.5
  475.0 0.9 convert_add_fusion.5
  476.0 0.9 convert_add_fusion.5
  477.0 0.9 convert_add_fusion.5
  478.0 0.9 convert_add_fusion.5
  479.0 0.9 convert_add_fusion.5
  480.0 0.9 convert_add_fusion.5
  481.9 0.9 convert_add_fusion.5
  483.9 0.9 convert_add_fusion.5
  484.9 0.9 convert_add_fusion.5
  486.9 0.9 convert_add_fusion.5
  487.9 0.9 convert_add_fusion.5
  489.9 0.9 convert_add_fusion.5
  491.8 0.9 convert_add_fusion.5
  492.8 0.9 convert_add_fusion.5
  494.8 0.9 convert_add_fusion.5
  495.8 0.9 convert_add_fusion.5
  497.8 0.9 convert_add_fusion.5
  499.3 2.4 reduce-window.6
  505.6 9.7 %all_to_all.25 = bf16[4,32,256]{2,1,0:T(8,128)(2,1)S(1)} all-to-all(bf16[4,32,256]{2,1,0:T(8,128)(2,1)S(1)} %convert_element_type.285), channel_id=1, replica_groups=mesh['sp'=32,'tp'=4,'dp'=8] {'tp'}, dimensions={0} | all-to-all | bytes 131072 | tf_op jit(solution)/shard_map/all_to_all | solution.py:305
  515.4 3.7 fusion.3
  (206 shorter events, 26.7 us)
Async XLA Ops:
  6.5 153.8 %copy-start = (bf16[2048,256]{1,0:T(8,128)(2,1)S(1)}, bf16[2048,256]{1,0:T(8,128)(2,1)}, u32[]{:S(2)}) copy-start(bf16[2048,256]{1,0:T(8,128)(2,1)} %param.28) | copy-start | bytes 3145732
  6.5 170.1 %copy-start.4 = (bf16[2,2048,4]{1,2,0:T(4,128)(2,1)S(1)}, bf16[2,2048,4]{1,2,0:T(4,128)(2,1)}, u32[]{:S(2)}) copy-start(bf16[2,2048,4]{1,2,0:T(4,128)(2,1)} %param.32) | copy-start | bytes 98308
  6.5 154.1 %copy-start.5 = (bf16[4,256]{1,0:T(4,128)(2,1)S(1)}, bf16[4,256]{1,0:T(4,128)(2,1)}, u32[]{:S(2)}) copy-start(bf16[4,256]{1,0:T(4,128)(2,1)} %param.33) | copy-start | bytes 6148
  6.5 170.6 %copy-start.2 = (bf16[2048,64]{0,1:T(8,128)(2,1)S(1)}, bf16[2048,64]{0,1:T(8,128)(2,1)}, u32[]{:S(2)}) copy-start(bf16[2048,64]{0,1:T(8,128)(2,1)} %param.30) | copy-start | bytes 786436
  6.5 154.1 %copy-start.6 = (bf16[4,64]{1,0:T(4,128)(2,1)S(1)}, bf16[4,64]{1,0:T(4,128)(2,1)}, u32[]{:S(2)}) copy-start(bf16[4,64]{1,0:T(4,128)(2,1)} %param.34) | copy-start | bytes 1540
  6.5 154.1 %copy-start.8 = (bf16[4,64]{1,0:T(4,128)(2,1)S(1)}, bf16[4,64]{1,0:T(4,128)(2,1)}, u32[]{:S(2)}) copy-start(bf16[4,64]{1,0:T(4,128)(2,1)} %param.35) | copy-start | bytes 1540
  6.6 154.3 %copy-start.9 = (f32[2,4]{1,0:T(2,128)S(1)}, f32[2,4]{1,0:T(2,128)}, u32[]{:S(2)}) copy-start(f32[2,4]{1,0:T(2,128)} %param.36) | copy-start | bytes 100
  6.6 154.3 %copy-start.10 = (bf16[256]{0:T(256)(128)(2,1)S(1)}, bf16[256]{0:T(256)(128)(2,1)}, u32[]{:S(2)}) copy-start(bf16[256]{0:T(256)(128)(2,1)} %param.38) | copy-start | bytes 1540
  150.4 27.7 %copy-start.7 = (f32[128,4]{0,1:T(4,128)S(1)}, f32[128,4]{0,1:T(4,128)}, u32[]{:S(2)}) copy-start(f32[128,4]{0,1:T(4,128)} %param.37) | copy-start | bytes 6148
  150.4 28.1 %copy-start.3 = (bf16[2048,64]{0,1:T(8,128)(2,1)S(1)}, bf16[2048,64]{0,1:T(8,128)(2,1)}, u32[]{:S(2)}) copy-start(bf16[2048,64]{0,1:T(8,128)(2,1)} %param.31) | copy-start | bytes 786436
  151.2 11.5 %all-to-all-start = ((bf16[4,32,2048]{2,1,0:T(8,128)(2,1)}), bf16[4,32,2048]{2,1,0:T(8,128)(2,1)S(1)}, u32[]{:S(2)}, u32[]{:S(2)}) async-start(bf16[4,32,2048]{2,1,0:T(8,128)(2,1)} %broadcast_in_dim.75), calls=%async_computation | async-start | bytes 1048576 | tf_op jit(solution)/shard_map/all_to_all | solution.py:49
  163.6 335.2 %all-to-all-start.1 = ((bf16[32,16,328]{2,1,0:T(8,128)(2,1)}), bf16[32,16,328]{2,1,0:T(8,128)(2,1)S(1)}, u32[]{:S(2)}, u32[]{:S(2)}) async-start(bf16[32,16,328]{2,1,0:T(8,128)(2,1)} %broadcast_in_dim.112), calls=%async_computation.1 | async-start | bytes 786432 | tf_op jit(solution)/shard_map/all_to_all | solution.py:49
  176.6 159.4 %all-gather.9.cloned.1.call-start = ((), (), s32[]{:S(2)}) async-start(), calls=%async_computation.3 | async-start | bytes 2162688 | tf_op jit(solution)/shard_map/all_gather | solution.py:23
  180.4 11.8 %collective-permute-start = (bf16[2,384]{0,1:T(8,128)(2,1)S(1)}, bf16[2,384]{0,1:T(8,128)(2,1)S(1)}, u32[]{:S(2)}, u32[]{:S(2)}) collective-permute-start(bf16[2,384]{0,1:T(8,128)(2,1)S(1)} %get-tuple-element.263), channel_id=1, source_target_pairs={{0,32},{32,64},{64,96},{96,128},{128,160},{160,192},{192,224},{224... | collective-permute-start | bytes 4616 | tf_op jit(solution)/shard_map/ppermute | solution.py:68
  184.2 11.1 %collective-permute-start.1 = (bf16[2,384]{0,1:T(8,128)(2,1)S(1)}, bf16[2,384]{0,1:T(8,128)(2,1)S(1)}, u32[]{:S(2)}, u32[]{:S(2)}) collective-permute-start(bf16[2,384]{0,1:T(8,128)(2,1)S(1)} %get-tuple-element.264), channel_id=1, source_target_pairs={{32,0},{64,32},{96,64},{128,96},{160,128},{192,160},{224,192},{256... | collective-permute-start | bytes 4616 | tf_op jit(solution)/shard_map/ppermute | solution.py:71
  196.7 271.3 %all-gather.11.cloned.1.call-start = ((), (), s32[]{:S(2)}) async-start(), calls=%async_computation.4 | async-start | bytes 2162688 | tf_op jit(solution)/shard_map/all_gather | solution.py:23
  502.8 12.6 %copy-start.1 = (bf16[32,2048]{1,0:T(8,128)(2,1)S(1)}, bf16[32,2048]{1,0:T(8,128)(2,1)}, u32[]{:S(2)}) copy-start(bf16[32,2048]{1,0:T(8,128)(2,1)} %param.22) | copy-start | bytes 393220
Sparse Core Ops, SparseCore 0:
  196.8 139.1 all-gather.8
  338.7 129.2 all-gather.10
where the time goes:
time: 528 us; the launch traced here: 526 us
  blocking collectives  259 us (49%)
  waiting for transfers between devices  167 us (32%)
  other arithmetic  40.5 us (8%)
  starting transfers between devices  21.6 us (4%)
  matrix products  15.3 us (3%)
  between operations  13.9 us (3%)
  local copies, waits for them, and re-layouts  7.19 us (1%)
    all_gather x2, waiting for transfers between devices, prefix(): lax.all_gather(a.astype(kind), axis)  156 us
    psum x2, blocking collectives, over_axes(): return functools.reduce(lax.psum, axes, x)  138 us
    all_gather x2, blocking collectives, prefix(): lax.all_gather(a.astype(kind), axis)  111 us
    add x31, other arithmetic, combine(): jnp.exp(later_part[0])[..., None, None] * earlier[1] + later_part[1]  28.9 us
    all_to_all x2, starting transfers between devices, from_everyone(): lax.all_to_all(jnp.broadcast_to(x[None], (length, *x.shape)), axis, 0, 0,...  16.5 us
  transfers between devices with their start and end apart: 6, of which 5 were waited for; matrix products, arithmetic and copies ran while one was open for 9% of the time, Pallas kernels for 0%

commit v1 on v0

v1 whole, which is shorter than its diff:
```python
import jax
import jax.numpy as jnp
import numpy as np
from jax import lax
from jax.sharding import Mesh
from jax.sharding import PartitionSpec as P

HEAD_DIM = 64
STATE = 64
ROW_EPS = 1e-06
GROUP_EPS = 1e-05
HIGHEST = lax.Precision.HIGHEST
F32 = jnp.float32
BF16 = jnp.bfloat16
PAD = 8

SP = ("za", "zb", "zc")
NEAR = ("zb", "zc")
MOD_NEAR = ("zc", "tp")
MOD_FAR = ("za", "zb")


def exchange(x, axis):
    return lax.all_to_all(x, axis, 0, 0, tiled=True)


def share(x, axis):
    n = lax.axis_size(axis)
    full = jnp.broadcast_to(x[None], (n, *x.shape)).reshape(n * x.shape[0], *x.shape[1:])
    return exchange(full, axis).reshape(n, *x.shape)


def split_hi_lo(x):
    hi = lax.reduce_precision(x, 8, 7)
    return hi, x - hi


def mod_vectors(cond, context_cond, modulation):
    share_rows = modulation.shape[0]
    width = modulation.shape[1] // 3
    rows = jax.nn.silu(jnp.stack([cond, context_cond]).astype(F32)).astype(BF16)
    own = lax.dynamic_slice_in_dim(rows, lax.axis_index((*SP, "tp")) * share_rows, share_rows, 1)
    part = jnp.dot(own, modulation, preferred_element_type=F32)
    n = lax.axis_size(MOD_NEAR)
    cut = width // n
    pairs = 5 * cut // 256
    part = part.reshape(6, n, cut)[:5].transpose(1, 0, 2).reshape(n * pairs, 2, 128)
    part = jnp.sum(exchange(part, MOD_NEAR).reshape(n, pairs, 2, 128), axis=0)
    part = jnp.sum(share(part, MOD_FAR), axis=0)
    full = share(part, MOD_NEAR)
    return full.reshape(n, 5, cut).transpose(1, 0, 2).reshape(5, width)


def modulated_norm(rows, norm_gain, shift_row, scale_row):
    values = rows.astype(F32)
    normed = values * lax.rsqrt(jnp.mean(values * values, axis=-1, keepdims=True) + ROW_EPS)
    return (normed * norm_gain.astype(F32) * (1.0 + scale_row) + shift_row).astype(BF16)


def conv(values, taps, first, length):
    total = jnp.zeros((length, values.shape[1]), F32)
    for k in range(4):
        total = total + taps[k].astype(F32) * values[first + k : first + k + length]
    return jax.nn.silu(total).astype(BF16)


def wide(v):
    heads = v.shape[1] // 2
    v = v.reshape(v.shape[0], 2, heads).transpose(0, 2, 1)
    return jnp.repeat(v, HEAD_DIM, axis=2).reshape(v.shape[0], heads * 2 * HEAD_DIM)


def twice(x):
    heads = x.shape[1] // HEAD_DIM
    v = x.reshape(x.shape[0], heads, 1, HEAD_DIM)
    return jnp.broadcast_to(v, (x.shape[0], heads, 2, HEAD_DIM)).reshape(x.shape[0], heads * 2 * HEAD_DIM)


def running_sums(log_decay):
    length = log_decay.shape[0]
    heads = log_decay.shape[1] // 2
    i = jnp.arange(length)
    low = (i[:, None] >= i[None, :]).astype(F32)
    forward = jnp.dot(low, log_decay[:, :heads], precision=HIGHEST)
    backward = jnp.dot(low.T, log_decay[:, heads:], precision=HIGHEST)
    return jnp.concatenate([forward, backward], axis=1)


def end_states(xs, bmat, dt, running, total):
    weights = wide(jnp.exp(total - running) * dt)
    weighted = (twice(xs).astype(F32) * weights).astype(BF16)
    return lax.dot_general(bmat, weighted, (((0,), (0,)), ((), ())), preferred_element_type=F32)


def before_products(totals, f_lane):
    run = jnp.cumsum(totals, axis=0)
    return jnp.where(f_lane, run[-1:] - run, run - totals)


def entry_states(ctx_state, ctx_total, lat_state, lat_total):
    heads = ctx_total.shape[1] // 2
    n = lax.axis_size(NEAR)
    half = heads * STATE // n

    def pieces(state):
        v = state.reshape(STATE // half, half, heads, 128).transpose(2, 0, 1, 3)
        return v.reshape(n, half, 128)

    decays = []
    for total in (ctx_total, lat_total):
        w = jnp.repeat(wide(total).reshape(heads, 1, 128), STATE // half, axis=0)
        decays += list(split_hi_lo(w))
    decays.append(jnp.zeros((n, 4, 128), F32))
    near = jnp.concatenate([pieces(ctx_state), pieces(lat_state), *decays], axis=1).astype(BF16)
    near = exchange(near, NEAR).astype(F32)
    f_lane = lax.broadcasted_iota(jnp.int32, (1, 128), 1) < HEAD_DIM
    group, member_total = [], None
    for k in range(2):
        states = near[:, k * half : (k + 1) * half]
        totals = near[:, 2 * half + 2 * k] + near[:, 2 * half + 2 * k + 1]
        group.append(jnp.sum(jnp.exp(before_products(totals, f_lane))[:, None] * states, axis=0))
        member_total = totals
        group.append(jnp.sum(totals, axis=0, keepdims=True))
    member_state = near[:, half : 2 * half]
    far = jnp.concatenate(
        [group[0], group[2], *split_hi_lo(group[1]), *split_hi_lo(group[3]), jnp.zeros((4, 128), F32)], axis=0
    ).astype(BF16)
    far = share(far, "za").astype(F32)
    count = far.shape[0]
    ctx_g, lat_g = far[:, :half], far[:, half : 2 * half]
    ctx_t = far[:, 2 * half] + far[:, 2 * half + 1]
    lat_t = far[:, 2 * half + 2] + far[:, 2 * half + 3]
    entry = jnp.sum(jnp.exp(before_products(ctx_t, f_lane))[:, None] * ctx_g, axis=0)
    place = lax.axis_index("za")
    for s in range(count - 1):
        keep = jnp.where(f_lane, s < place, count - 1 - s > place)
        total = jnp.where(f_lane, lat_t[s], lat_t[count - 1 - s])
        state = jnp.where(f_lane, lat_g[s], lat_g[count - 1 - s])
        entry = jnp.where(keep, jnp.exp(total) * entry + state, entry)
    entries = [entry]
    for s in range(n - 1):
        total = jnp.where(f_lane, member_total[s], member_total[n - 1 - s])
        state = jnp.where(f_lane, member_state[s], member_state[n - 1 - s])
        entry = jnp.exp(total) * entry + state
        entries.append(entry)
    back = jnp.stack([jnp.where(f_lane, entries[m], entries[n - 1 - m]) for m in range(n)]).astype(BF16)
    back = exchange(back, NEAR)
    return back.reshape(heads, STATE, 128)


def local(
    latent,
    cond,
    context,
    context_cond,
    modulation,
    norm_gain,
    w_x,
    w_gate,
    w_b,
    w_c,
    w_dt,
    conv_x,
    conv_b,
    conv_c,
    decay_rate,
    decay_extra,
    out_gain,
    w_out,
):
    heads = w_dt.shape[2]
    head_cols = w_x.shape[1]
    tokens = decay_extra.shape[0]
    ctx_tokens = context.shape[0]
    mods = mod_vectors(cond, context_cond, modulation)

    block = share(latent, "tp").reshape(tokens, latent.shape[1])
    count = lax.axis_size(SP)
    place = lax.axis_index(SP)
    up = [(i, i + 1) for i in range(count - 1)]
    down = [(i + 1, i) for i in range(count - 1)]
    low = lax.ppermute(jnp.concatenate([block[-PAD:], context[-PAD:]]), SP, up)
    high = lax.ppermute(jnp.concatenate([block[:PAD], context[:PAD]]), SP, down)
    latent_rows = jnp.concatenate([low[:PAD], block, high[:PAD]])
    context_rows = jnp.concatenate([low[PAD:], context, high[PAD:]])

    lat_len = tokens + 2 * PAD
    hidden = jnp.concatenate(
        [
            modulated_norm(latent_rows, norm_gain, mods[0], mods[1]),
            modulated_norm(context_rows, norm_gain, mods[3], mods[4]),
        ]
    )
    row = jnp.arange(hidden.shape[0])
    first = (row < PAD) | ((row >= lat_len) & (row < lat_len + PAD))
    last = ((row >= lat_len - PAD) & (row < lat_len)) | (row >= hidden.shape[0] - PAD)
    outside = (first & (place == 0)) | (last & (place == count - 1))
    inner = hidden[PAD : PAD + tokens]

    def project(rows, weight):
        return jnp.dot(rows, weight, preferred_element_type=F32).astype(BF16)

    p_x = jnp.where(outside[:, None], 0.0, project(hidden, w_x).astype(F32))
    p_b = jnp.where(outside[:, None], 0.0, project(hidden, w_b).astype(F32))
    p_c = jnp.where(outside[:lat_len, None], 0.0, project(hidden[:lat_len], w_c).astype(F32))
    p_dt = jax.nn.softplus(project(hidden, jnp.concatenate([w_dt[0], w_dt[1]], axis=1)).astype(F32))
    z = project(inner, w_gate).astype(F32)

    off = PAD - 2
    xs = conv(p_x, conv_x, off, tokens)
    bmat = conv(p_b, conv_b, off, tokens)
    cmat = conv(p_c, conv_c, off, tokens)
    ctx_xs = conv(p_x, conv_x, lat_len + off, ctx_tokens)
    ctx_b = conv(p_b, conv_b, lat_len + off, ctx_tokens)
    dt = p_dt[PAD : PAD + tokens]
    ctx_dt = p_dt[lat_len + PAD : lat_len + PAD + ctx_tokens]
    rate = decay_rate.reshape(1, 2 * heads)
    log_decay = -rate * dt + jnp.concatenate([decay_extra, decay_extra], axis=1)
    ctx_log_decay = -rate * ctx_dt
    running = running_sums(log_decay)
    ctx_running = running_sums(ctx_log_decay)
    total = jnp.sum(log_decay, axis=0, keepdims=True)
    ctx_total = jnp.sum(ctx_log_decay, axis=0, keepdims=True)
    entry = entry_states(
        end_states(ctx_xs, ctx_b, ctx_dt, ctx_running, ctx_total),
        ctx_total,
        end_states(xs, bmat, dt, running, total),
        total,
    )

    affinity = lax.dot_general(cmat, bmat, (((1,), (1,)), ((), ())), preferred_element_type=F32)
    i = jnp.arange(tokens)
    lower = i[:, None] >= i[None, :]
    upper = i[:, None] <= i[None, :]
    parts = []
    for h in range(heads):
        weights = jnp.zeros((tokens, tokens), F32)
        for d, mask in ((0, lower), (1, upper)):
            col = d * heads + h
            gap = running[:, col][:, None] - running[:, col][None, :]
            mixing = jnp.where(mask, jnp.exp(jnp.where(mask, gap, 0.0)), 0.0)
            weights = weights + mixing * dt[:, col][None, :]
        weights = (affinity * weights).astype(BF16)
        parts.append(jnp.dot(weights, xs[:, h * HEAD_DIM : (h + 1) * HEAD_DIM], preferred_element_type=F32))
    y = jnp.concatenate(parts, axis=1)
    flat = entry.transpose(1, 0, 2).reshape(STATE, heads * 128)
    carried = jnp.dot(cmat, flat, preferred_element_type=F32) * wide(jnp.exp(running))
    carried = carried.reshape(tokens, heads, 2, HEAD_DIM)
    y = y + (carried[:, :, 0] + carried[:, :, 1]).reshape(tokens, heads * HEAD_DIM)
    gated = y * jax.nn.silu(z)
    mean_square = jnp.mean(gated * gated, axis=1, keepdims=True)
    normed = (gated * lax.rsqrt(mean_square + GROUP_EPS) * out_gain.astype(F32)).astype(BF16)
    tp_count = lax.axis_size("tp")
    stacked = normed.reshape(tp_count, tokens // tp_count, head_cols)
    full = lax.all_to_all(stacked, "tp", split_axis=0, concat_axis=2, tiled=True)[0]
    branch = jnp.dot(full, w_out, preferred_element_type=F32)
    return (latent.astype(F32) + mods[2] * branch).astype(BF16)


def solution(mesh):
    sp, tp, dp = (mesh.shape[a] for a in ("sp", "tp", "dp"))
    inner = Mesh(np.asarray(mesh.devices).reshape(sp // 8, 4, 2, tp, dp), (*SP, "tp", "dp"))
    in_specs = (
        P(("dp", *SP, "tp"), None),
        P("dp"),
        P(("dp", *SP), None),
        P(),
        P((*SP, "tp"), None),
        P(),
        P(None, "tp"),
        P(None, "tp"),
        P(None, "tp"),
        P(None, "tp"),
        P(None, None, "tp"),
        P(None, "tp"),
        P(None, "tp"),
        P(None, "tp"),
        P(None, "tp"),
        P(("dp", *SP), "tp"),
        P("tp"),
        P(),
    )
    out_specs = P(("dp", *SP, "tp"), None)
    return jax.shard_map(local, mesh=inner, in_specs=in_specs, out_specs=out_specs, check_vma=False)
```

time: 528 us -> 182 us (0.34)
  the two profiles are of different devices: /device:TPU:2 before, /device:TPU:4 now
where the time goes in v1:
time: 182 us; the launch traced here: 181 us
  waiting for transfers between devices  77.1 us (42%)
  starting transfers between devices  60.8 us (33%)
  other arithmetic  11.7 us (6%)
  matrix products  11.6 us (6%)
  local copies, waits for them, and re-layouts  11.1 us (6%)
  blocking collectives  7.99 us (4%)
    all_to_all x7, waiting for transfers between devices, exchange(): return lax.all_to_all(x, axis, 0, 0, tiled=True)  71.4 us
    all_to_all x7, starting transfers between devices, exchange(): return lax.all_to_all(x, axis, 0, 0, tiled=True)  56.1 us
    all_to_all x1, blocking collectives, local(): lax.all_to_all(stacked, 'tp', split_axis=0, concat_axis=2, tiled=True)[0]  7.99 us
    ppermute x1, waiting for transfers between devices, local(): high = lax.ppermute(jnp.concatenate([block[:PAD], context[:PAD]]), SP, down)  4.41 us
    unnamed x7, other arithmetic  4.27 us
    dot_general x1, matrix products, local(): branch = jnp.dot(full, w_out, preferred_element_type=F32)  3.68 us
    broadcast_in_dim x4, local copies, waits for them, and re-layouts, share(): jnp.broadcast_to(x[None], (n, *x.shape))  3.67 us
  transfers between devices with their start and end apart: 9, of which 9 were waited for; matrix products, arithmetic and copies ran while one was open for 5% of the time, Pallas kernels for 0%

profile of v1, /device:TPU:4, one launch (start us, length us, event | category | flops | bytes accessed | tf_op | source)
XLA Modules:
  0.0 180.8 jit_solution(8614415746756026583)
XLA Ops:
  0.0 0.8 stack.10
  0.8 0.7 stack.9
  1.5 1.2 fusion.116
  2.8 0.6 reshape.1536
  3.4 5.8 %all-to-all-start = ((f32[40,2,128]{2,1,0:T(2,128)}), f32[40,2,128]{2,1,0:T(2,128)S(1)}, u32[]{:S(2)}, u32[]{:S(2)}) async-start(f32[40,2,128]{2,1,0:T(2,128)} %reshape.1536), calls=%async_computation | async-start | bytes 81920 | tf_op jit(solution)/shard_map/all_to_all | solution.py:24
  9.3 0.8 fusion.145
  10.0 0.7 convert_element_type.170
  10.7 0.8 bitcast_convert_fusion.3
  11.6 0.8 bitcast_convert_fusion.7
  12.4 0.7 neg.45
  13.2 0.7 convert_element_type.203
  13.9 0.8 slice_convert_fusion.3
  14.7 0.8 all-to-all-done
  15.5 1.7 broadcast_in_dim.345
  17.3 4.1 %all-to-all-start.3 = ((bf16[4,32,2048]{2,1,0:T(8,128)(2,1)}), bf16[4,32,2048]{2,1,0:T(8,128)(2,1)S(1)}, u32[]{:S(2)}, u32[]{:S(2)}) async-start(bf16[4,32,2048]{2,1,0:T(8,128)(2,1)} %broadcast_in_dim.345), calls=%async_computation.3 | async-start | bytes 1048576 | tf_op jit(solution)/shard_map/all_to_all | solution.py:24
  21.4 8.9 %all-to-all-done.3 = bf16[4,32,2048]{2,1,0:T(8,128)(2,1)S(1)} async-done(((bf16[4,32,2048]{2,1,0:T(8,128)(2,1)}), bf16[4,32,2048]{2,1,0:T(8,128)(2,1)S(1)}, u32[]{:S(2)}, u32[]{:S(2)}) %all-to-all-start.3) | async-done | bytes 524320 | tf_op jit(solution)/shard_map/all_to_all | solution.py:24
  30.3 0.7 broadcast_in_dim.341
  30.9 27.5 %all-to-all-start.1 = ((f32[80,2,128]{2,1,0:T(2,128)}), f32[80,2,128]{2,1,0:T(2,128)S(1)}, u32[]{:S(2)}, u32[]{:S(2)}) async-start(f32[80,2,128]{2,1,0:T(2,128)} %bitcast.2), calls=%async_computation.1 | async-start | bytes 163840 | tf_op jit(solution)/shard_map/all_to_all | solution.py:24
  58.5 3.4 %collective-permute-start = (bf16[16,2048]{1,0:T(8,128)(2,1)S(1)}, bf16[16,2048]{1,0:T(8,128)(2,1)S(1)}, u32[]{:S(2)}, u32[]{:S(2)}) collective-permute-start(bf16[16,2048]{1,0:T(8,128)(2,1)S(1)} %pad_maximum_fusion.6), channel_id=1, source_target_pairs={{0,32},{32,64},{64,96},{96,128},{128,160},{160,192},{192,224},{224... | collective-permute-start | bytes 196616 | tf_op jit(solution)/shard_map/ppermute | solution.py:182
  61.9 1.3 collective-permute-start.1
  63.2 1.2 collective-permute-done
  64.5 4.4 %collective-permute-done.1 = bf16[16,2048]{1,0:T(8,128)(2,1)S(1)} collective-permute-done((bf16[16,2048]{1,0:T(8,128)(2,1)S(1)}, bf16[16,2048]{1,0:T(8,128)(2,1)S(1)}, u32[]{:S(2)}, u32[]{:S(2)}) %collective-permute-start.1) | collective-permute-done | bytes 65568 | tf_op jit(solution)/shard_map/ppermute | solution.py:183
  69.0 14.3 %all-to-all-done.1 = f32[80,2,128]{2,1,0:T(2,128)S(1)} async-done(((f32[80,2,128]{2,1,0:T(2,128)}), f32[80,2,128]{2,1,0:T(2,128)S(1)}, u32[]{:S(2)}, u32[]{:S(2)}) %all-to-all-start.1) | async-done | bytes 81952 | tf_op jit(solution)/shard_map/all_to_all | solution.py:24
  83.3 0.6 broadcast_in_dim.342
  84.0 3.3 %all-to-all-start.2 = ((f32[40,2,128]{2,1,0:T(2,128)}), f32[40,2,128]{2,1,0:T(2,128)S(1)}, u32[]{:S(2)}, u32[]{:S(2)}) async-start(f32[40,2,128]{2,1,0:T(2,128)} %bitcast.4), calls=%async_computation.2 | async-start | bytes 81920 | tf_op jit(solution)/shard_map/all_to_all | solution.py:24
  87.5 6.0 %all-to-all-done.2 = f32[40,2,128]{2,1,0:T(2,128)S(1)} async-done(((f32[40,2,128]{2,1,0:T(2,128)}), f32[40,2,128]{2,1,0:T(2,128)S(1)}, u32[]{:S(2)}, u32[]{:S(2)}) %all-to-all-start.2) | async-done | bytes 40992 | tf_op jit(solution)/shard_map/all_to_all | solution.py:24
  98.5 1.9 %concatenate.59 = bf16[8,72,128]{2,1,0:T(8,128)(2,1)} concatenate(bf16[8,32,128]{2,1,0:T(8,128)(2,1)S(1)} %bitcast.303, bf16[8,32,128]{2,1,0:T(8,128)(2,1)S(1)} %bitcast.302, bf16[8,1,128]{2,1,0:T(2,128)(2,1)S(1)} %copy.171, bf16[8,1,128]{2,1,0:T(2,128)(2,1)S(1)} %copy.172, bf16[8,1,128]{2,1,0:T(2,128)(2,1)S(1)} %copy.173, bf16[8,1,128]{2,1,0:T(2,128)(2,1)S(1)} %copy.174, ...), dimensions={1} | concatenate | bytes 294912 | tf_op jit(solution)/shard_map/concatenate | solution.py:114
  100.4 3.4 %all-to-all-start.4 = ((bf16[8,72,128]{2,1,0:T(8,128)(2,1)}), bf16[8,72,128]{2,1,0:T(8,128)(2,1)S(1)}, u32[]{:S(2)}, u32[]{:S(2)}) async-start(bf16[8,72,128]{2,1,0:T(8,128)(2,1)} %concatenate.59), calls=%async_computation.4 | async-start | bytes 294912 | tf_op jit(solution)/shard_map/all_to_all | solution.py:24
  104.6 10.8 %all-to-all-done.4 = bf16[8,72,128]{2,1,0:T(8,128)(2,1)S(1)} async-done(((bf16[8,72,128]{2,1,0:T(8,128)(2,1)}), bf16[8,72,128]{2,1,0:T(8,128)(2,1)S(1)}, u32[]{:S(2)}, u32[]{:S(2)}) %all-to-all-start.4) | async-done | bytes 147488 | tf_op jit(solution)/shard_map/all_to_all | solution.py:24
  115.6 0.6 broadcast_in_dim.370
  116.3 8.0 %all-to-all-start.5 = ((bf16[4,72,128]{2,1,0:T(8,128)(2,1)}), bf16[4,72,128]{2,1,0:T(8,128)(2,1)S(1)}, u32[]{:S(2)}, u32[]{:S(2)}) async-start(bf16[4,72,128]{2,1,0:T(8,128)(2,1)} %broadcast_in_dim.370), calls=%async_computation.5 | async-start | bytes 147456 | tf_op jit(solution)/shard_map/all_to_all | solution.py:24
  124.3 0.9 fusion.46
  125.2 21.7 %all-to-all-done.5 = bf16[4,72,128]{2,1,0:T(8,128)(2,1)S(1)} async-done(((bf16[4,72,128]{2,1,0:T(8,128)(2,1)}), bf16[4,72,128]{2,1,0:T(8,128)(2,1)S(1)}, u32[]{:S(2)}, u32[]{:S(2)}) %all-to-all-start.5) | async-done | bytes 73760 | tf_op jit(solution)/shard_map/all_to_all | solution.py:24
  147.0 0.6 constant_dynamic-update-slice_fusion.7
  147.7 0.6 constant_dynamic-update-slice_fusion.6
  148.3 0.6 constant_dynamic-update-slice_fusion.5
  148.9 0.6 constant_dynamic-update-slice_fusion.4
  149.5 0.6 constant_dynamic-update-slice_fusion.3
  150.1 0.6 constant_dynamic-update-slice_fusion.2
  150.7 0.6 constant_dynamic-update-slice_fusion.1
  151.3 0.6 constant_dynamic-update-slice_fusion
  151.9 3.9 %all-to-all-start.6 = ((bf16[8,32,128]{2,1,0:T(8,128)(2,1)}), bf16[8,32,128]{2,1,0:T(8,128)(2,1)S(1)}, u32[]{:S(2)}, u32[]{:S(2)}) async-start(bf16[8,32,128]{2,1,0:T(8,128)(2,1)} %constant_dynamic-update-slice_fusion), calls=%async_computation.6 | async-start | bytes 131072 | tf_op jit(solution)/shard_map/all_to_all | solution.py:24
  156.0 0.9 fusion.44
  156.9 0.9 fusion.42
  157.7 9.0 %all-to-all-done.6 = bf16[8,32,128]{2,1,0:T(8,128)(2,1)S(1)} async-done(((bf16[8,32,128]{2,1,0:T(8,128)(2,1)}), bf16[8,32,128]{2,1,0:T(8,128)(2,1)S(1)}, u32[]{:S(2)}, u32[]{:S(2)}) %all-to-all-start.6) | async-done | bytes 65568 | tf_op jit(solution)/shard_map/all_to_all | solution.py:24
  167.6 1.3 multiply_reduce_fusion
  169.1 8.0 %all_to_all.55 = bf16[4,32,256]{2,1,0:T(8,128)(2,1)S(1)} all-to-all(bf16[4,32,256]{2,1,0:T(8,128)(2,1)S(1)} %bitcast.305), channel_id=1, replica_groups=mesh['za'=4,'zb'=4,'zc'=2,'tp'=4,'dp'=8] {'tp'}, dimensions={0} | all-to-all | bytes 131072 | tf_op jit(solution)/shard_map/all_to_all | solution.py:255
  177.2 3.7 %fusion.1 = bf16[32,2048]{1,0:T(8,128)(2,1)} fusion(bf16[32,1024]{1,0:T(8,128)(2,1)S(1)} %bitcast.301, bf16[1024,2048]{1,0:T(8,128)(2,1)} %param.35, bf16[32,2048]{1,0:T(8,128)(2,1)S(1)} %copy-done.2, f32[2048]{0:T(1024)S(1)} %bitcast.316), kind=kOutput, calls=%fused_computation.2 | convolution fusion | flops 134479872 | bytes 4530176 | tf_op jit(solution)/shard_map/dot_general | solution.py:256
  (127 shorter events, 7.8 us)
Async XLA Ops:
  0.0 94.8 %copy-start = (bf16[2048,256]{1,0:T(8,128)(2,1)S(1)}, bf16[2048,256]{1,0:T(8,128)(2,1)}, u32[]{:S(2)}) copy-start(bf16[2048,256]{1,0:T(8,128)(2,1)} %param.24) | copy-start | bytes 3145732
  2.7 18.7 %copy-start.4 = (bf16[2,2048,4]{1,2,0:T(4,128)(2,1)S(1)}, bf16[2,2048,4]{1,2,0:T(4,128)(2,1)}, u32[]{:S(2)}) copy-start(bf16[2,2048,4]{1,2,0:T(4,128)(2,1)} %param.28) | copy-start | bytes 98308
  3.4 12.1 %all-to-all-start = ((f32[40,2,128]{2,1,0:T(2,128)}), f32[40,2,128]{2,1,0:T(2,128)S(1)}, u32[]{:S(2)}, u32[]{:S(2)}) async-start(f32[40,2,128]{2,1,0:T(2,128)} %reshape.1536), calls=%async_computation | async-start | bytes 81920 | tf_op jit(solution)/shard_map/all_to_all | solution.py:24
  17.3 51.6 %copy-start.1 = (bf16[16,2048]{1,0:T(8,128)(2,1)S(1)}, bf16[16,2048]{1,0:T(8,128)(2,1)}, u32[]{:S(2)}) copy-start(bf16[16,2048]{1,0:T(8,128)(2,1)} %param.20) | copy-start | bytes 196612
  17.3 13.0 %all-to-all-start.3 = ((bf16[4,32,2048]{2,1,0:T(8,128)(2,1)}), bf16[4,32,2048]{2,1,0:T(8,128)(2,1)S(1)}, u32[]{:S(2)}, u32[]{:S(2)}) async-start(bf16[4,32,2048]{2,1,0:T(8,128)(2,1)} %broadcast_in_dim.345), calls=%async_computation.3 | async-start | bytes 1048576 | tf_op jit(solution)/shard_map/all_to_all | solution.py:24
  30.9 52.4 %all-to-all-start.1 = ((f32[80,2,128]{2,1,0:T(2,128)}), f32[80,2,128]{2,1,0:T(2,128)S(1)}, u32[]{:S(2)}, u32[]{:S(2)}) async-start(f32[80,2,128]{2,1,0:T(2,128)} %bitcast.2), calls=%async_computation.1 | async-start | bytes 163840 | tf_op jit(solution)/shard_map/all_to_all | solution.py:24
  58.5 5.9 %collective-permute-start = (bf16[16,2048]{1,0:T(8,128)(2,1)S(1)}, bf16[16,2048]{1,0:T(8,128)(2,1)S(1)}, u32[]{:S(2)}, u32[]{:S(2)}) collective-permute-start(bf16[16,2048]{1,0:T(8,128)(2,1)S(1)} %pad_maximum_fusion.6), channel_id=1, source_target_pairs={{0,32},{32,64},{64,96},{96,128},{128,160},{160,192},{192,224},{224... | collective-permute-start | bytes 196616 | tf_op jit(solution)/shard_map/ppermute | solution.py:182
  61.9 7.0 %collective-permute-start.1 = (bf16[16,2048]{1,0:T(8,128)(2,1)S(1)}, bf16[16,2048]{1,0:T(8,128)(2,1)S(1)}, u32[]{:S(2)}, u32[]{:S(2)}) collective-permute-start(bf16[16,2048]{1,0:T(8,128)(2,1)S(1)} %pad_maximum_fusion.7), channel_id=1, source_target_pairs={{32,0},{64,32},{96,64},{128,96},{160,128},{192,160},{224,192},{256... | collective-permute-start | bytes 196616 | tf_op jit(solution)/shard_map/ppermute | solution.py:183
  84.0 9.6 %all-to-all-start.2 = ((f32[40,2,128]{2,1,0:T(2,128)}), f32[40,2,128]{2,1,0:T(2,128)S(1)}, u32[]{:S(2)}, u32[]{:S(2)}) async-start(f32[40,2,128]{2,1,0:T(2,128)} %bitcast.4), calls=%async_computation.2 | async-start | bytes 81920 | tf_op jit(solution)/shard_map/all_to_all | solution.py:24
  93.6 0.8 copy-start.5
  94.8 1.0 copy-start.7
  96.2 7.6 %copy-start.3 = (bf16[2048,64]{0,1:T(8,128)(2,1)S(1)}, bf16[2048,64]{0,1:T(8,128)(2,1)}, u32[]{:S(2)}) copy-start(bf16[2048,64]{0,1:T(8,128)(2,1)} %param.27) | copy-start | bytes 786436
  100.4 15.0 %all-to-all-start.4 = ((bf16[8,72,128]{2,1,0:T(8,128)(2,1)}), bf16[8,72,128]{2,1,0:T(8,128)(2,1)S(1)}, u32[]{:S(2)}, u32[]{:S(2)}) async-start(bf16[8,72,128]{2,1,0:T(8,128)(2,1)} %concatenate.59), calls=%async_computation.4 | async-start | bytes 294912 | tf_op jit(solution)/shard_map/all_to_all | solution.py:24
  116.3 30.6 %all-to-all-start.5 = ((bf16[4,72,128]{2,1,0:T(8,128)(2,1)}), bf16[4,72,128]{2,1,0:T(8,128)(2,1)S(1)}, u32[]{:S(2)}, u32[]{:S(2)}) async-start(bf16[4,72,128]{2,1,0:T(8,128)(2,1)} %broadcast_in_dim.370), calls=%async_computation.5 | async-start | bytes 147456 | tf_op jit(solution)/shard_map/all_to_all | solution.py:24
  151.9 14.8 %all-to-all-start.6 = ((bf16[8,32,128]{2,1,0:T(8,128)(2,1)}), bf16[8,32,128]{2,1,0:T(8,128)(2,1)S(1)}, u32[]{:S(2)}, u32[]{:S(2)}) async-start(bf16[8,32,128]{2,1,0:T(8,128)(2,1)} %constant_dynamic-update-slice_fusion), calls=%async_computation.6 | async-start | bytes 131072 | tf_op jit(solution)/shard_map/all_to_all | solution.py:24
  156.9 10.4 %copy-start.6 = (bf16[2048,256]{1,0:T(8,128)(2,1)S(1)}, bf16[2048,256]{1,0:T(8,128)(2,1)}, u32[]{:S(2)}) copy-start(bf16[2048,256]{1,0:T(8,128)(2,1)} %param.25) | copy-start | bytes 3145732
  166.8 0.8 copy-start.8
  167.6 9.5 %copy-start.2 = (bf16[32,2048]{1,0:T(8,128)(2,1)S(1)}, bf16[32,2048]{1,0:T(8,128)(2,1)}, u32[]{:S(2)}) copy-start(bf16[32,2048]{1,0:T(8,128)(2,1)} %param.18) | copy-start | bytes 393220

commit v2 on v1

--- a/solution.py
+++ b/solution.py
@@ -4,6 +4,7 @@
 from jax import lax
 from jax.sharding import Mesh
 from jax.sharding import PartitionSpec as P
+
 
 HEAD_DIM = 64
 STATE = 64
@@ -30,12 +31,20 @@
     return exchange(full, axis).reshape(n, *x.shape)
 
 
+def ring_rows(x):
+    n = lax.axis_size("tp")
+    moved = [x] + [lax.ppermute(x, "tp", [(i, (i + k) % n) for i in range(n)]) for k in range(1, n)]
+    moved = jnp.stack(moved)
+    place = lax.axis_index("tp")
+    return jnp.stack([lax.dynamic_index_in_dim(moved, (place - t) % n, 0, False) for t in range(n)])
+
+
 def split_hi_lo(x):
     hi = lax.reduce_precision(x, 8, 7)
     return hi, x - hi
 
 
-def mod_vectors(cond, context_cond, modulation):
+def mod_vectors(cond, context_cond, modulation, own_rows):
     share_rows = modulation.shape[0]
     width = modulation.shape[1] // 3
     rows = jax.nn.silu(jnp.stack([cond, context_cond]).astype(F32)).astype(BF16)
@@ -46,9 +55,11 @@
     pairs = 5 * cut // 256
     part = part.reshape(6, n, cut)[:5].transpose(1, 0, 2).reshape(n * pairs, 2, 128)
     part = jnp.sum(exchange(part, MOD_NEAR).reshape(n, pairs, 2, 128), axis=0)
-    part = jnp.sum(share(part, MOD_FAR), axis=0)
-    full = share(part, MOD_NEAR)
-    return full.reshape(n, 5, cut).transpose(1, 0, 2).reshape(5, width)
+    part, own_rows = lax.optimization_barrier((part, own_rows))
+    far = share(part, MOD_FAR)
+    gathered = ring_rows(own_rows)
+    full = share(jnp.sum(far, axis=0), MOD_NEAR)
+    return full.reshape(n, 5, cut).transpose(1, 0, 2).reshape(5, width), gathered
 
 
 def modulated_norm(rows, norm_gain, shift_row, scale_row):
@@ -92,9 +103,19 @@
     return lax.dot_general(bmat, weighted, (((0,), (0,)), ((), ())), preferred_element_type=F32)
 
 
-def before_products(totals, f_lane):
-    run = jnp.cumsum(totals, axis=0)
-    return jnp.where(f_lane, run[-1:] - run, run - totals)
+def entry_sums(states, totals, f_lane):
+    n = states.shape[0]
+    m = lax.broadcasted_iota(jnp.int32, (n + 1, n, n, 1), 0)
+    k = lax.broadcasted_iota(jnp.int32, (n + 1, n, n, 1), 1)
+    j = lax.broadcasted_iota(jnp.int32, (n + 1, n, n, 1), 2)
+    mb = jnp.where(m == n, -1, m)
+    between = jnp.where(f_lane, (j > k) & (j < m), (j < k) & (j > mb))
+    gap = jnp.sum(jnp.where(between, totals[None, None], 0.0), axis=2)
+    ahead = jnp.where(f_lane, k[:, :, 0] < m[:, :, 0], k[:, :, 0] > mb[:, :, 0])
+    factor = jnp.where(ahead, jnp.exp(gap), 0.0)
+    sums = jnp.sum(factor[:, :, None] * states[None], axis=1)
+    to_m = jnp.sum(jnp.where(ahead, totals[None], 0.0), axis=1)
+    return sums, to_m
 
 
 def entry_states(ctx_state, ctx_total, lat_state, lat_total):
@@ -114,41 +135,27 @@
     near = jnp.concatenate([pieces(ctx_state), pieces(lat_state), *decays], axis=1).astype(BF16)
     near = exchange(near, NEAR).astype(F32)
     f_lane = lax.broadcasted_iota(jnp.int32, (1, 128), 1) < HEAD_DIM
-    group, member_total = [], None
-    for k in range(2):
-        states = near[:, k * half : (k + 1) * half]
-        totals = near[:, 2 * half + 2 * k] + near[:, 2 * half + 2 * k + 1]
-        group.append(jnp.sum(jnp.exp(before_products(totals, f_lane))[:, None] * states, axis=0))
-        member_total = totals
-        group.append(jnp.sum(totals, axis=0, keepdims=True))
-    member_state = near[:, half : 2 * half]
+    ctx_t = near[:, 2 * half] + near[:, 2 * half + 1]
+    lat_t = near[:, 2 * half + 2] + near[:, 2 * half + 3]
+    ctx_sums, ctx_to = entry_sums(near[:, :half], ctx_t, f_lane)
+    lat_sums, lat_to = entry_sums(near[:, half : 2 * half], lat_t, f_lane)
     far = jnp.concatenate(
-        [group[0], group[2], *split_hi_lo(group[1]), *split_hi_lo(group[3]), jnp.zeros((4, 128), F32)], axis=0
+        [ctx_sums[n], lat_sums[n], *split_hi_lo(ctx_to[n:]), *split_hi_lo(lat_to[n:]), jnp.zeros((4, 128), F32)], axis=0
     ).astype(BF16)
     far = share(far, "za").astype(F32)
     count = far.shape[0]
-    ctx_g, lat_g = far[:, :half], far[:, half : 2 * half]
-    ctx_t = far[:, 2 * half] + far[:, 2 * half + 1]
-    lat_t = far[:, 2 * half + 2] + far[:, 2 * half + 3]
-    entry = jnp.sum(jnp.exp(before_products(ctx_t, f_lane))[:, None] * ctx_g, axis=0)
-    place = lax.axis_index("za")
-    for s in range(count - 1):
-        keep = jnp.where(f_lane, s < place, count - 1 - s > place)
-        total = jnp.where(f_lane, lat_t[s], lat_t[count - 1 - s])
-        state = jnp.where(f_lane, lat_g[s], lat_g[count - 1 - s])
-        entry = jnp.where(keep, jnp.exp(total) * entry + state, entry)
-    entries = [entry]
-    for s in range(n - 1):
-        total = jnp.where(f_lane, member_total[s], member_total[n - 1 - s])
-        state = jnp.where(f_lane, member_state[s], member_state[n - 1 - s])
-        entry = jnp.exp(total) * entry + state
-        entries.append(entry)
-    back = jnp.stack([jnp.where(f_lane, entries[m], entries[n - 1 - m]) for m in range(n)]).astype(BF16)
+    start, _ = entry_sums(far[:, :half], far[:, 2 * half] + far[:, 2 * half + 1], f_lane)
+    group, group_to = entry_sums(far[:, half : 2 * half], far[:, 2 * half + 2] + far[:, 2 * half + 3], f_lane)
+    mine = (jnp.arange(count + 1) == lax.axis_index("za")).astype(F32)
+    group = jnp.sum(mine[:, None, None] * group, axis=0)
+    group_to = jnp.sum(mine[:, None] * group_to, axis=0)
+    entry = jnp.exp(group_to) * start[count] + group
+    back = (jnp.exp(lat_to[:n, None]) * entry + lat_sums[:n]).astype(BF16)
     back = exchange(back, NEAR)
     return back.reshape(heads, STATE, 128)
 
 
-def local(
+def program(
     latent,
     cond,
     context,
@@ -172,16 +179,22 @@
     head_cols = w_x.shape[1]
     tokens = decay_extra.shape[0]
     ctx_tokens = context.shape[0]
-    mods = mod_vectors(cond, context_cond, modulation)
-
-    block = share(latent, "tp").reshape(tokens, latent.shape[1])
     count = lax.axis_size(SP)
     place = lax.axis_index(SP)
     up = [(i, i + 1) for i in range(count - 1)]
     down = [(i + 1, i) for i in range(count - 1)]
-    low = lax.ppermute(jnp.concatenate([block[-PAD:], context[-PAD:]]), SP, up)
-    high = lax.ppermute(jnp.concatenate([block[:PAD], context[:PAD]]), SP, down)
-    latent_rows = jnp.concatenate([low[:PAD], block, high[:PAD]])
+    low = lax.ppermute(jnp.concatenate([latent[-PAD:], context[-PAD:]]), SP, up)
+    high = lax.ppermute(jnp.concatenate([latent[:PAD], context[:PAD]]), SP, down)
+    own = jnp.concatenate([latent, low[:PAD], high[:PAD]])
+    mods, gathered = mod_vectors(cond, context_cond, modulation, own)
+    tokens_own = latent.shape[0]
+    latent_rows = jnp.concatenate(
+        [
+            gathered[-1, tokens_own : tokens_own + PAD],
+            gathered[:, :tokens_own].reshape(tokens, latent.shape[1]),
+            gathered[0, tokens_own + PAD :],
+        ]
+    )
     context_rows = jnp.concatenate([low[PAD:], context, high[PAD:]])
 
     lat_len = tokens + 2 * PAD
@@ -281,4 +294,4 @@
         P(),
     )
     out_specs = P(("dp", *SP, "tp"), None)
-    return jax.shard_map(local, mesh=inner, in_specs=in_specs, out_specs=out_specs, check_vma=False)
+    return jax.shard_map(program, mesh=inner, in_specs=in_specs, out_specs=out_specs, check_vma=False)

time: 182 us -> 178 us (0.978)
  starting transfers between devices: 60.8 us -> 71.6 us
  other arithmetic: 11.7 us -> 4.19 us
  waiting for transfers between devices: 77.1 us -> 72.8 us
    ppermute x2 -> x5, starting transfers between devices: 4.66 us -> 16.5 us  [the longest x3 10.7 us: ring_rows(): lax.ppermute(x, 'tp', [(i, (i + k) % n) for i in range(n)])]
    ppermute x2 -> x5, waiting for transfers between devices: 5.66 us -> 0.88 us  [the longest x1 0.87 us: program(): low = lax.ppermute(jnp.concatenate([latent[-PAD:], context[-PAD:]]), SP, up)]
    unnamed x7 -> x0, other arithmetic: 4.27 us -> none
    mul x3, other arithmetic: 2.5 us -> 0.02 us  [conv(): total = total + taps[k].astype(F32) * values[first + k:first + k + length]]
    dot_general x7, matrix products: 6.82 us -> 4.95 us  [the longest x1 3.68 us: program(): branch = jnp.dot(full, w_out, preferred_element_type=F32)]
    broadcast_in_dim x4 -> x3, local copies, waits for them, and re-layouts: 3.67 us -> 1.93 us  [share(): jnp.broadcast_to(x[None], (n, *x.shape))]
    all_to_all x7 -> x6, starting transfers between devices: 56.1 us -> 55.1 us  [exchange(): return lax.all_to_all(x, axis, 0, 0, tiled=True)]
    all_to_all x7 -> x6, waiting for transfers between devices: 71.4 us -> 71.9 us  [exchange(): return lax.all_to_all(x, axis, 0, 0, tiled=True)]
  transfers between devices with their start and end apart: 9 -> 11, of which waited for: 9 -> 6; matrix products, arithmetic and copies ran while one was open for 5% -> 3% of each run, Pallas kernels for 0% -> 0%
where the time goes in v2:
time: 178 us; the launch traced here: 177 us
  waiting for transfers between devices  72.8 us (41%)
  starting transfers between devices  71.6 us (40%)
  matrix products  10 us (6%)
  local copies, waits for them, and re-layouts  9.47 us (5%)
  blocking collectives  7.99 us (4%)
  other arithmetic  4.19 us (2%)
    all_to_all x6, waiting for transfers between devices, exchange(): return lax.all_to_all(x, axis, 0, 0, tiled=True)  71.9 us
    all_to_all x6, starting transfers between devices, exchange(): return lax.all_to_all(x, axis, 0, 0, tiled=True)  55.1 us
    ppermute x3, starting transfers between devices, ring_rows(): lax.ppermute(x, 'tp', [(i, (i + k) % n) for i in range(n)])  10.7 us
    all_to_all x1, blocking collectives, program(): lax.all_to_all(stacked, 'tp', split_axis=0, concat_axis=2, tiled=True)[0]  7.99 us
    ppermute x1, starting transfers between devices, program(): low = lax.ppermute(jnp.concatenate([latent[-PAD:], context[-PAD:]]), SP, up)  4.56 us
    dot_general x1, matrix products, program(): branch = jnp.dot(full, w_out, preferred_element_type=F32)  3.68 us
  transfers between devices with their start and end apart: 11, of which 6 were waited for; matrix products, arithmetic and copies ran while one was open for 3% of the time, Pallas kernels for 0%

profile of v2, /device:TPU:4, one launch (start us, length us, event | category | flops | bytes accessed | tf_op | source)
XLA Modules:
  0.0 176.9 jit_solution(18018603290002713589)
XLA Ops:
  0.1 0.8 stack.32
  0.9 0.7 stack.31
  1.6 1.2 fusion.129
  2.8 0.6 reshape.566
  3.5 5.8 %all-to-all-start = ((f32[40,2,128]{2,1,0:T(2,128)}), f32[40,2,128]{2,1,0:T(2,128)S(1)}, u32[]{:S(2)}, u32[]{:S(2)}) async-start(f32[40,2,128]{2,1,0:T(2,128)} %reshape.566), calls=%async_computation | async-start | bytes 81920 | tf_op jit(solution)/shard_map/all_to_all | solution.py:25
  9.3 0.8 fusion.145
  10.1 1.3 collective-permute-start.1
  11.5 4.6 %collective-permute-start = (bf16[16,2048]{1,0:T(8,128)(2,1)S(1)}, bf16[16,2048]{1,0:T(8,128)(2,1)S(1)}, u32[]{:S(2)}, u32[]{:S(2)}) collective-permute-start(bf16[16,2048]{1,0:T(8,128)(2,1)S(1)} %pad_maximum_fusion.11), channel_id=1, source_target_pairs={{0,32},{32,64},{64,96},{96,128},{128,160},{160,192},{192,224},{224... | collective-permute-start | bytes 196616 | tf_op jit(solution)/shard_map/ppermute | solution.py:186
  17.0 0.9 collective-permute-done
  18.1 5.1 %collective-permute-start.4 = (bf16[48,2048]{1,0:T(8,128)(2,1)S(1)}, bf16[48,2048]{1,0:T(8,128)(2,1)S(1)}, u32[]{:S(2)}, u32[]{:S(2)}) collective-permute-start(bf16[48,2048]{1,0:T(8,128)(2,1)S(1)} %pad_maximum_fusion.9), channel_id=1, source_target_pairs={{0,24},{8,0},{16,8},{24,16},{1,25},{9,1},{17,9},{25,17},{2,26},{10... | collective-permute-start | bytes 589832 | tf_op jit(solution)/shard_map/ppermute | solution.py:36
  23.3 2.8 %collective-permute-start.3 = (bf16[48,2048]{1,0:T(8,128)(2,1)S(1)}, bf16[48,2048]{1,0:T(8,128)(2,1)S(1)}, u32[]{:S(2)}, u32[]{:S(2)}) collective-permute-start(bf16[48,2048]{1,0:T(8,128)(2,1)S(1)} %pad_maximum_fusion.9), channel_id=1, source_target_pairs={{0,16},{8,24},{16,0},{24,8},{1,17},{9,25},{17,1},{25,9},{2,18},{10... | collective-permute-start | bytes 589832 | tf_op jit(solution)/shard_map/ppermute | solution.py:36
  26.0 2.8 %collective-permute-start.2 = (bf16[48,2048]{1,0:T(8,128)(2,1)S(1)}, bf16[48,2048]{1,0:T(8,128)(2,1)S(1)}, u32[]{:S(2)}, u32[]{:S(2)}) collective-permute-start(bf16[48,2048]{1,0:T(8,128)(2,1)S(1)} %pad_maximum_fusion.9), channel_id=1, source_target_pairs={{0,8},{8,16},{16,24},{24,0},{1,9},{9,17},{17,25},{25,1},{2,10},{10... | collective-permute-start | bytes 589832 | tf_op jit(solution)/shard_map/ppermute | solution.py:36
  28.8 0.7 broadcast_in_dim.439
  29.5 29.6 %all-to-all-start.1 = ((f32[80,2,128]{2,1,0:T(2,128)}), f32[80,2,128]{2,1,0:T(2,128)S(1)}, u32[]{:S(2)}, u32[]{:S(2)}) async-start(f32[80,2,128]{2,1,0:T(2,128)} %bitcast.2), calls=%async_computation.1 | async-start | bytes 163840 | tf_op jit(solution)/shard_map/all_to_all | solution.py:25
  59.4 22.3 %all-to-all-done.1 = f32[80,2,128]{2,1,0:T(2,128)S(1)} async-done(((f32[80,2,128]{2,1,0:T(2,128)}), f32[80,2,128]{2,1,0:T(2,128)S(1)}, u32[]{:S(2)}, u32[]{:S(2)}) %all-to-all-start.1) | async-done | bytes 81952 | tf_op jit(solution)/shard_map/all_to_all | solution.py:25
  81.8 0.6 broadcast_in_dim.440
  82.4 3.7 %all-to-all-start.2 = ((f32[40,2,128]{2,1,0:T(2,128)}), f32[40,2,128]{2,1,0:T(2,128)S(1)}, u32[]{:S(2)}, u32[]{:S(2)}) async-start(f32[40,2,128]{2,1,0:T(2,128)} %bitcast.4), calls=%async_computation.2 | async-start | bytes 81920 | tf_op jit(solution)/shard_map/all_to_all | solution.py:25
  86.1 0.2 fusion.2
  86.3 6.1 %all-to-all-done.2 = f32[40,2,128]{2,1,0:T(2,128)S(1)} async-done(((f32[40,2,128]{2,1,0:T(2,128)}), f32[40,2,128]{2,1,0:T(2,128)S(1)}, u32[]{:S(2)}, u32[]{:S(2)}) %all-to-all-start.2) | async-done | bytes 40992 | tf_op jit(solution)/shard_map/all_to_all | solution.py:25
  92.4 0.3 fusion.6
  92.9 0.3 compare_select_fusion
  93.2 0.2 fusion.142
  93.5 0.2 fusion.41
  93.7 0.2 fusion.143
  94.2 0.3 fusion.11
  94.6 0.4 fusion.8
  95.9 0.2 fusion.13
  96.5 0.2 fusion.12
  97.3 1.9 %concatenate.67 = bf16[8,72,128]{2,1,0:T(8,128)(2,1)} concatenate(bf16[8,32,128]{2,1,0:T(8,128)(2,1)S(1)} %bitcast.214, bf16[8,32,128]{2,1,0:T(8,128)(2,1)S(1)} %bitcast.215, bf16[8,1,128]{2,1,0:T(2,128)(2,1)S(1)} %copy.216, bf16[8,1,128]{2,1,0:T(2,128)(2,1)S(1)} %copy.217, bf16[8,1,128]{2,1,0:T(2,128)(2,1)S(1)} %copy.218, bf16[8,1,128]{2,1,0:T(2,128)(2,1)S(1)} %copy.219, ...), dimensions={1} | concatenate | bytes 294912 | tf_op jit(solution)/shard_map/concatenate | solution.py:135
  99.2 4.2 %all-to-all-start.3 = ((bf16[8,72,128]{2,1,0:T(8,128)(2,1)}), bf16[8,72,128]{2,1,0:T(8,128)(2,1)S(1)}, u32[]{:S(2)}, u32[]{:S(2)}) async-start(bf16[8,72,128]{2,1,0:T(8,128)(2,1)} %concatenate.67), calls=%async_computation.3 | async-start | bytes 294912 | tf_op jit(solution)/shard_map/all_to_all | solution.py:25
  103.4 0.3 fusion.15
  103.8 0.2 fusion.151
  104.0 0.2 fusion.48
  104.2 10.8 %all-to-all-done.3 = bf16[8,72,128]{2,1,0:T(8,128)(2,1)S(1)} async-done(((bf16[8,72,128]{2,1,0:T(8,128)(2,1)}), bf16[8,72,128]{2,1,0:T(8,128)(2,1)S(1)}, u32[]{:S(2)}, u32[]{:S(2)}) %all-to-all-start.3) | async-done | bytes 147488 | tf_op jit(solution)/shard_map/all_to_all | solution.py:25
  115.1 0.3 fusion.18
  115.8 0.6 broadcast_in_dim.480
  116.5 7.9 %all-to-all-start.4 = ((bf16[4,72,128]{2,1,0:T(8,128)(2,1)}), bf16[4,72,128]{2,1,0:T(8,128)(2,1)S(1)}, u32[]{:S(2)}, u32[]{:S(2)}) async-start(bf16[4,72,128]{2,1,0:T(8,128)(2,1)} %broadcast_in_dim.480), calls=%async_computation.4 | async-start | bytes 147456 | tf_op jit(solution)/shard_map/all_to_all | solution.py:25
  124.3 0.2 fusion.50
  124.6 22.5 %all-to-all-done.4 = bf16[4,72,128]{2,1,0:T(8,128)(2,1)S(1)} async-done(((bf16[4,72,128]{2,1,0:T(8,128)(2,1)}), bf16[4,72,128]{2,1,0:T(8,128)(2,1)S(1)}, u32[]{:S(2)}, u32[]{:S(2)}) %all-to-all-start.4) | async-done | bytes 73760 | tf_op jit(solution)/shard_map/all_to_all | solution.py:25
  147.6 0.6 fusion.25
  148.2 3.9 %all-to-all-start.5 = ((bf16[8,32,128]{2,1,0:T(8,128)(2,1)}), bf16[8,32,128]{2,1,0:T(8,128)(2,1)S(1)}, u32[]{:S(2)}, u32[]{:S(2)}) async-start(bf16[8,32,128]{2,1,0:T(8,128)(2,1)} %fusion.25), calls=%async_computation.5 | async-start | bytes 131072 | tf_op jit(solution)/shard_map/all_to_all | solution.py:25
  152.3 0.2 fusion.52
  152.5 0.2 fusion.54
  152.8 10.2 %all-to-all-done.5 = bf16[8,32,128]{2,1,0:T(8,128)(2,1)S(1)} async-done(((bf16[8,32,128]{2,1,0:T(8,128)(2,1)}), bf16[8,32,128]{2,1,0:T(8,128)(2,1)S(1)}, u32[]{:S(2)}, u32[]{:S(2)}) %all-to-all-start.5) | async-done | bytes 65568 | tf_op jit(solution)/shard_map/all_to_all | solution.py:25
  163.0 0.2 convolution_multiply_fusion.1
  163.4 1.6 multiply_reduce_fusion.4
  165.2 8.0 %all_to_all.46 = bf16[4,32,256]{2,1,0:T(8,128)(2,1)S(1)} all-to-all(bf16[4,32,256]{2,1,0:T(8,128)(2,1)S(1)} %bitcast.217), channel_id=1, replica_groups=mesh['za'=4,'zb'=4,'zc'=2,'tp'=4,'dp'=8] {'tp'}, dimensions={0} | all-to-all | bytes 131072 | tf_op jit(solution)/shard_map/all_to_all | solution.py:268
  173.3 3.7 %fusion.1 = bf16[32,2048]{1,0:T(8,128)(2,1)} fusion(bf16[32,1024]{1,0:T(8,128)(2,1)S(1)} %bitcast.213, bf16[1024,2048]{1,0:T(8,128)(2,1)} %param.35, bf16[32,2048]{1,0:T(8,128)(2,1)S(1)} %copy-done.1, f32[2048]{0:T(1024)S(1)} %bitcast.231), kind=kOutput, calls=%fused_computation.2 | convolution fusion | flops 134479872 | bytes 4530176 | tf_op jit(solution)/shard_map/dot_general | solution.py:269
  (151 shorter events, 5.4 us)
Async XLA Ops:
  0.0 94.6 %copy-start = (bf16[2048,256]{1,0:T(8,128)(2,1)S(1)}, bf16[2048,256]{1,0:T(8,128)(2,1)}, u32[]{:S(2)}) copy-start(bf16[2048,256]{1,0:T(8,128)(2,1)} %param.24) | copy-start | bytes 3145732
  0.0 18.1 %copy-start.1 = (bf16[32,2048]{1,0:T(8,128)(2,1)S(1)}, bf16[32,2048]{1,0:T(8,128)(2,1)}, u32[]{:S(2)}) copy-start(bf16[32,2048]{1,0:T(8,128)(2,1)} %param.18) | copy-start | bytes 393220
  0.0 17.9 %copy-start.2 = (bf16[16,2048]{1,0:T(8,128)(2,1)S(1)}, bf16[16,2048]{1,0:T(8,128)(2,1)}, u32[]{:S(2)}) copy-start(bf16[16,2048]{1,0:T(8,128)(2,1)} %param.20) | copy-start | bytes 196612
  0.0 16.3 %copy-start.6 = (bf16[2048]{0:T(1024)(128)(2,1)S(1)}, bf16[2048]{0:T(1024)(128)(2,1)}, u32[]{:S(2)}) copy-start(bf16[2048]{0:T(1024)(128)(2,1)} %param.23) | copy-start | bytes 12292
  0.0 16.4 %copy-start.4 = (bf16[2,2048,4]{1,2,0:T(4,128)(2,1)S(1)}, bf16[2,2048,4]{1,2,0:T(4,128)(2,1)}, u32[]{:S(2)}) copy-start(bf16[2,2048,4]{1,2,0:T(4,128)(2,1)} %param.28) | copy-start | bytes 98308
  0.0 16.4 %copy-start.10 = (f32[2,4]{1,0:T(2,128)S(1)}, f32[2,4]{1,0:T(2,128)}, u32[]{:S(2)}) copy-start(f32[2,4]{1,0:T(2,128)} %param.32) | copy-start | bytes 100
  0.0 16.5 %copy-start.7 = (bf16[4,64]{1,0:T(4,128)(2,1)S(1)}, bf16[4,64]{1,0:T(4,128)(2,1)}, u32[]{:S(2)}) copy-start(bf16[4,64]{1,0:T(4,128)(2,1)} %param.31) | copy-start | bytes 1540
  0.1 16.5 %copy-start.8 = (bf16[4,64]{1,0:T(4,128)(2,1)S(1)}, bf16[4,64]{1,0:T(4,128)(2,1)}, u32[]{:S(2)}) copy-start(bf16[4,64]{1,0:T(4,128)(2,1)} %param.30) | copy-start | bytes 1540
  0.1 16.5 %copy-start.5 = (bf16[4,256]{1,0:T(4,128)(2,1)S(1)}, bf16[4,256]{1,0:T(4,128)(2,1)}, u32[]{:S(2)}) copy-start(bf16[4,256]{1,0:T(4,128)(2,1)} %param.29) | copy-start | bytes 6148
  0.1 16.9 %copy-start.12 = (bf16[256]{0:T(256)(128)(2,1)S(1)}, bf16[256]{0:T(256)(128)(2,1)}, u32[]{:S(2)}) copy-start(bf16[256]{0:T(256)(128)(2,1)} %param.34) | copy-start | bytes 1540
  3.5 14.6 %all-to-all-start = ((f32[40,2,128]{2,1,0:T(2,128)}), f32[40,2,128]{2,1,0:T(2,128)S(1)}, u32[]{:S(2)}, u32[]{:S(2)}) async-start(f32[40,2,128]{2,1,0:T(2,128)} %reshape.566), calls=%async_computation | async-start | bytes 81920 | tf_op jit(solution)/shard_map/all_to_all | solution.py:25
  10.1 6.9 %collective-permute-start.1 = (bf16[16,2048]{1,0:T(8,128)(2,1)S(1)}, bf16[16,2048]{1,0:T(8,128)(2,1)S(1)}, u32[]{:S(2)}, u32[]{:S(2)}) collective-permute-start(bf16[16,2048]{1,0:T(8,128)(2,1)S(1)} %pad_maximum_fusion.12), channel_id=1, source_target_pairs={{32,0},{64,32},{96,64},{128,96},{160,128},{192,160},{224,192},{256... | collective-permute-start | bytes 196616 | tf_op jit(solution)/shard_map/ppermute | solution.py:187
  11.5 6.5 %collective-permute-start = (bf16[16,2048]{1,0:T(8,128)(2,1)S(1)}, bf16[16,2048]{1,0:T(8,128)(2,1)S(1)}, u32[]{:S(2)}, u32[]{:S(2)}) collective-permute-start(bf16[16,2048]{1,0:T(8,128)(2,1)S(1)} %pad_maximum_fusion.11), channel_id=1, source_target_pairs={{0,32},{32,64},{64,96},{96,128},{128,160},{160,192},{192,224},{224... | collective-permute-start | bytes 196616 | tf_op jit(solution)/shard_map/ppermute | solution.py:186
  18.1 41.0 %collective-permute-start.4 = (bf16[48,2048]{1,0:T(8,128)(2,1)S(1)}, bf16[48,2048]{1,0:T(8,128)(2,1)S(1)}, u32[]{:S(2)}, u32[]{:S(2)}) collective-permute-start(bf16[48,2048]{1,0:T(8,128)(2,1)S(1)} %pad_maximum_fusion.9), channel_id=1, source_target_pairs={{0,24},{8,0},{16,8},{24,16},{1,25},{9,1},{17,9},{25,17},{2,26},{10... | collective-permute-start | bytes 589832 | tf_op jit(solution)/shard_map/ppermute | solution.py:36
  23.3 35.9 %collective-permute-start.3 = (bf16[48,2048]{1,0:T(8,128)(2,1)S(1)}, bf16[48,2048]{1,0:T(8,128)(2,1)S(1)}, u32[]{:S(2)}, u32[]{:S(2)}) collective-permute-start(bf16[48,2048]{1,0:T(8,128)(2,1)S(1)} %pad_maximum_fusion.9), channel_id=1, source_target_pairs={{0,16},{8,24},{16,0},{24,8},{1,17},{9,25},{17,1},{25,9},{2,18},{10... | collective-permute-start | bytes 589832 | tf_op jit(solution)/shard_map/ppermute | solution.py:36
  26.0 33.1 %collective-permute-start.2 = (bf16[48,2048]{1,0:T(8,128)(2,1)S(1)}, bf16[48,2048]{1,0:T(8,128)(2,1)S(1)}, u32[]{:S(2)}, u32[]{:S(2)}) collective-permute-start(bf16[48,2048]{1,0:T(8,128)(2,1)S(1)} %pad_maximum_fusion.9), channel_id=1, source_target_pairs={{0,8},{8,16},{16,24},{24,0},{1,9},{9,17},{17,25},{25,1},{2,10},{10... | collective-permute-start | bytes 589832 | tf_op jit(solution)/shard_map/ppermute | solution.py:36
  29.5 52.2 %all-to-all-start.1 = ((f32[80,2,128]{2,1,0:T(2,128)}), f32[80,2,128]{2,1,0:T(2,128)S(1)}, u32[]{:S(2)}, u32[]{:S(2)}) async-start(f32[80,2,128]{2,1,0:T(2,128)} %bitcast.2), calls=%async_computation.1 | async-start | bytes 163840 | tf_op jit(solution)/shard_map/all_to_all | solution.py:25
  82.4 9.9 %all-to-all-start.2 = ((f32[40,2,128]{2,1,0:T(2,128)}), f32[40,2,128]{2,1,0:T(2,128)S(1)}, u32[]{:S(2)}, u32[]{:S(2)}) async-start(f32[40,2,128]{2,1,0:T(2,128)} %bitcast.4), calls=%async_computation.2 | async-start | bytes 81920 | tf_op jit(solution)/shard_map/all_to_all | solution.py:25
  92.4 0.8 copy-start.9
  92.4 1.7 copy-start.11
  95.1 8.3 %copy-start.3 = (bf16[2048,64]{0,1:T(8,128)(2,1)S(1)}, bf16[2048,64]{0,1:T(8,128)(2,1)}, u32[]{:S(2)}) copy-start(bf16[2048,64]{0,1:T(8,128)(2,1)} %param.27) | copy-start | bytes 786436
  99.2 15.8 %all-to-all-start.3 = ((bf16[8,72,128]{2,1,0:T(8,128)(2,1)}), bf16[8,72,128]{2,1,0:T(8,128)(2,1)S(1)}, u32[]{:S(2)}, u32[]{:S(2)}) async-start(bf16[8,72,128]{2,1,0:T(8,128)(2,1)} %concatenate.67), calls=%async_computation.3 | async-start | bytes 294912 | tf_op jit(solution)/shard_map/all_to_all | solution.py:25
  116.5 30.5 %all-to-all-start.4 = ((bf16[4,72,128]{2,1,0:T(8,128)(2,1)}), bf16[4,72,128]{2,1,0:T(8,128)(2,1)S(1)}, u32[]{:S(2)}, u32[]{:S(2)}) async-start(bf16[4,72,128]{2,1,0:T(8,128)(2,1)} %broadcast_in_dim.480), calls=%async_computation.4 | async-start | bytes 147456 | tf_op jit(solution)/shard_map/all_to_all | solution.py:25
  148.2 14.8 %all-to-all-start.5 = ((bf16[8,32,128]{2,1,0:T(8,128)(2,1)}), bf16[8,32,128]{2,1,0:T(8,128)(2,1)S(1)}, u32[]{:S(2)}, u32[]{:S(2)}) async-start(bf16[8,32,128]{2,1,0:T(8,128)(2,1)} %fusion.25), calls=%async_computation.5 | async-start | bytes 131072 | tf_op jit(solution)/shard_map/all_to_all | solution.py:25

commit v3 on v2

v3 whole, which is shorter than its diff:
```python
import jax
import jax.numpy as jnp
import numpy as np
from jax import lax
from jax.experimental import pallas as pl
from jax.experimental.pallas import tpu as pltpu
from jax.sharding import Mesh
from jax.sharding import PartitionSpec as P


HEAD_DIM = 64
STATE = 64
ROW_EPS = 1e-06
GROUP_EPS = 1e-05
HIGHEST = lax.Precision.HIGHEST
F32 = jnp.float32
BF16 = jnp.bfloat16
PAD = 8

SP = ("za", "zb", "zc")
NEAR = ("zb", "zc")
MOD_NEAR = ("zc", "tp")
MOD_FAR = ("za", "zb")


def exchange(x, axis):
    return lax.all_to_all(x, axis, 0, 0, tiled=True)


def share(x, axis):
    n = lax.axis_size(axis)
    full = jnp.broadcast_to(x[None], (n, *x.shape)).reshape(n * x.shape[0], *x.shape[1:])
    return exchange(full, axis).reshape(n, *x.shape)


def ring_rows(x):
    n = lax.axis_size("tp")
    moved = [x] + [lax.ppermute(x, "tp", [(i, (i + k) % n) for i in range(n)]) for k in range(1, n)]
    moved = jnp.stack(moved)
    place = lax.axis_index("tp")
    return jnp.stack([lax.dynamic_index_in_dim(moved, (place - t) % n, 0, False) for t in range(n)])


def split_hi_lo(x):
    hi = lax.reduce_precision(x, 8, 7)
    return hi, x - hi


def silu(v):
    return v / (1.0 + jnp.exp(-v))


def partial_kernel(first, cond, context_cond, modulation, out):
    share_rows, cols = modulation.shape
    width = cols // 3
    at = first[0] + lax.broadcasted_iota(jnp.int32, (share_rows, width), 0)
    pick = jnp.where(lax.broadcasted_iota(jnp.int32, (share_rows, width), 1) == at, 1.0, 0.0).astype(BF16)
    table = modulation[...]
    cut = width // (out.shape[0] // 5)
    for source, kinds in ((0, (0, 1, 2)), (1, (0, 1))):
        v = (cond, context_cond)[source][...].astype(F32)
        row = silu(v).astype(BF16)
        own = lax.dot_general(row, pick, (((1,), (1,)), ((), ())), preferred_element_type=F32).astype(BF16)
        sums = jnp.dot(own, table, preferred_element_type=F32)
        for kind in kinds:
            for n in range(width // cut):
                for r in range(2):
                    at = kind * width + n * cut + r * 128
                    out[n * 5 + 3 * source + kind, r : r + 1, :] = sums[0:1, at : at + 128]


def partial_mods(first, cond, context_cond, modulation, n):
    vmem = pl.BlockSpec(memory_space=pltpu.VMEM)
    width = modulation.shape[1] // 3
    return pl.pallas_call(
        partial_kernel,
        out_shape=jax.ShapeDtypeStruct((n * 5, 2, 128), F32),
        in_specs=[pl.BlockSpec(memory_space=pltpu.SMEM), vmem, vmem, vmem],
        out_specs=vmem,
        compiler_params=pltpu.CompilerParams(vmem_limit_bytes=8 * 2**20),
        name="partial_mods",
    )(
        first.astype(jnp.int32).reshape(1),
        jnp.broadcast_to(cond[None], (8, width)),
        jnp.broadcast_to(context_cond[None], (8, width)),
        modulation,
    )


def mod_vectors(cond, context_cond, modulation, own_rows):
    share_rows = modulation.shape[0]
    width = modulation.shape[1] // 3
    n = lax.axis_size(MOD_NEAR)
    pairs = 5 * (width // n) // 256
    first = lax.axis_index((*SP, "tp")) * share_rows
    part = partial_mods(first, cond, context_cond, modulation, n)
    part = jnp.sum(exchange(part, MOD_NEAR).reshape(n, pairs, 2, 128), axis=0)
    part, own_rows = lax.optimization_barrier((part, own_rows))
    far = share(part, MOD_FAR)
    gathered = ring_rows(own_rows)
    full = share(jnp.sum(far, axis=0), MOD_NEAR)
    return full.reshape(n * pairs, 2, 128), gathered


def wide(v):
    heads = v.shape[1] // 2
    v = v.reshape(v.shape[0], 2, heads).transpose(0, 2, 1)
    return jnp.repeat(v, HEAD_DIM, axis=2).reshape(v.shape[0], heads * 2 * HEAD_DIM)


def front_kernel(
    edge, rows, mods, gain, w_dt, taps, rate, extra, w_x, w_g, w_bc,
    near, xs_out, bc_out, z_out, run_out, dt_out, gate_out,
    hid, buf_x, buf_g, buf_bc, proj, sems,
):
    copies = [
        pltpu.make_async_copy(src, dst, sems.at[i])
        for i, (src, dst) in enumerate(((w_x, buf_x), (w_bc, buf_bc), (w_g, buf_g)))
    ]
    for c in copies:
        c.start()
    total_rows, _ = rows.shape
    tokens = xs_out.shape[0]
    lat_rows = tokens + 2 * PAD
    ctx = total_rows - lat_rows - 2 * PAD
    chunks = mods.shape[0] // 5

    def vector(kind):
        return jnp.concatenate([mods[n * 5 + kind, r : r + 1, :] for n in range(chunks) for r in range(2)], axis=1)

    gate_out[...] = vector(2)
    g = gain[...].astype(F32)
    for first, count, shift, scale in ((0, lat_rows, 0, 1), (lat_rows, total_rows - lat_rows, 3, 4)):
        shift_row = vector(shift)
        factor = g * (1.0 + vector(scale))

        def norm(i, _, first=first, shift_row=shift_row, factor=factor):
            at = pl.ds(pl.multiple_of(first + i * 16, 16), 16)
            v = rows[at, :].astype(F32)
            r = lax.rsqrt(jnp.mean(v * v, axis=1, keepdims=True) + ROW_EPS)
            hid[at, :] = (v * r * factor + shift_row).astype(BF16)
            return 0

        lax.fori_loop(0, count // 16, norm, 0)

    def rounded(v):
        return v.astype(BF16).astype(F32)

    hidden = hid[...]
    p_dt = lax.dot_general(hidden, w_dt[...], (((1,), (1,)), ((), ())), preferred_element_type=F32)
    copies[0].wait()
    p_x = rounded(jnp.dot(hidden, buf_x[...], preferred_element_type=F32))
    copies[1].wait()
    p_bc = rounded(jnp.dot(hidden, buf_bc[...], preferred_element_type=F32))
    row = lax.broadcasted_iota(jnp.int32, (total_rows, 1), 0)
    is_first = (row < PAD) | ((row >= lat_rows) & (row < lat_rows + PAD))
    is_last = ((row >= lat_rows - PAD) & (row < lat_rows)) | (row >= total_rows - PAD)
    outside = (is_first & (edge[0] == 1)) | (is_last & (edge[1] == 1))
    cols = p_x.shape[1]
    proj[:, :cols] = jnp.where(outside, 0.0, p_x)
    proj[:, cols:] = jnp.where(outside, 0.0, p_bc)

    def conv(first, length):
        acc = jnp.zeros((length, proj.shape[1]), F32)
        for k in range(4):
            acc = acc + taps[k : k + 1, :].astype(F32) * proj[first + k : first + k + length, :]
        return silu(acc).astype(BF16)

    lat_u = conv(PAD - 2, tokens)
    ctx_u = conv(lat_rows + PAD - 2, ctx)
    xs_out[...] = lat_u[:, :cols]
    bc_out[...] = lat_u[:, cols:]
    v = rounded(p_dt)
    p_dt = jnp.maximum(v, 0.0) + jnp.log1p(jnp.exp(-jnp.abs(v)))
    heads = extra.shape[1] // 2
    lane = lax.broadcasted_iota(jnp.int32, (1, 128), 1) < HEAD_DIM
    slots = near.shape[0]
    half = heads * STATE // slots
    rows8 = lax.broadcasted_iota(jnp.int32, (8, 1), 0)
    decays = []
    for u, dt, more, base in (
        (ctx_u, p_dt[lat_rows + PAD : lat_rows + PAD + ctx], None, 0),
        (lat_u, p_dt[PAD : PAD + tokens], extra, half),
    ):
        length = dt.shape[0]
        log_decay = -rate[...] * dt
        if more is not None:
            log_decay = log_decay + more[...]
        i = lax.broadcasted_iota(jnp.int32, (length, length), 0)
        j = lax.broadcasted_iota(jnp.int32, (length, length), 1)
        low = jnp.where(i >= j, 1.0, 0.0)
        high = jnp.where(i <= j, 1.0, 0.0)
        ahead = lax.broadcasted_iota(jnp.int32, (1, 2 * heads), 1) < heads
        running = jnp.where(
            ahead,
            jnp.dot(low, log_decay, precision=HIGHEST, preferred_element_type=F32),
            jnp.dot(high, log_decay, precision=HIGHEST, preferred_element_type=F32),
        )
        total = jnp.sum(log_decay, axis=0, keepdims=True)
        weight = jnp.exp(total - running) * dt
        if more is not None:
            run_out[...] = running
            dt_out[...] = dt
        bmat = u[:, cols : cols + STATE]
        here = []
        for h in range(heads):
            pair = u[:, 128 * (h // 2) : 128 * (h // 2) + 128].astype(F32)
            other = pltpu.roll(pair, HEAD_DIM, 1)
            twice = jnp.where(lane, pair, other) if h % 2 == 0 else jnp.where(lane, other, pair)
            w = jnp.where(lane, weight[:, h : h + 1], weight[:, heads + h : heads + h + 1])
            state = lax.dot_general(
                bmat, (twice * w).astype(BF16), (((0,), (0,)), ((), ())), preferred_element_type=F32
            ).astype(BF16)
            for part in range(STATE // half):
                near[h * (STATE // half) + part, base : base + half, :] = state[part * half : (part + 1) * half]
            here.append(jnp.where(lane, total[:, h : h + 1], total[:, heads + h : heads + h + 1]))
        decays.append(here)
    for h in range(heads):
        block = jnp.zeros((8, 128), F32)
        for k in range(2):
            t = decays[k][h]
            hi = rounded(t)
            block = jnp.where(rows8 == 2 * k, hi, jnp.where(rows8 == 2 * k + 1, t - hi, block))
        block = block.astype(BF16)
        for part in range(STATE // half):
            near[h * (STATE // half) + part, 2 * half :, :] = block
    copies[2].wait()
    z = rounded(jnp.dot(hid[PAD : PAD + tokens, :], buf_g[...], preferred_element_type=F32))
    z_out[...] = silu(z)


def front(edge, rows, mods, gain, w_dt, taps, rate, extra, w_x, w_g, w_bc, slots):
    tokens, heads2 = extra.shape
    cols = w_x.shape[1]
    width = rows.shape[1]
    vmem = pl.BlockSpec(memory_space=pltpu.VMEM)
    away = pl.BlockSpec(memory_space=pl.ANY)
    half = heads2 // 2 * STATE // slots
    shape = jax.ShapeDtypeStruct
    return pl.pallas_call(
        front_kernel,
        out_shape=(
            shape((slots, 2 * half + 8, 128), BF16),
            shape((tokens, cols), BF16),
            shape((tokens, w_bc.shape[1]), BF16),
            shape((tokens, cols), F32),
            shape((tokens, heads2), F32),
            shape((tokens, heads2), F32),
            shape((1, width), F32),
        ),
        in_specs=[pl.BlockSpec(memory_space=pltpu.SMEM)] + [vmem] * 7 + [away] * 3,
        out_specs=(vmem,) * 7,
        scratch_shapes=[
            pltpu.VMEM(rows.shape, BF16),
            pltpu.VMEM(w_x.shape, BF16),
            pltpu.VMEM(w_g.shape, BF16),
            pltpu.VMEM(w_bc.shape, BF16),
            pltpu.VMEM((rows.shape[0], cols + w_bc.shape[1]), F32),
            pltpu.SemaphoreType.DMA((3,)),
        ],
        compiler_params=pltpu.CompilerParams(vmem_limit_bytes=24 * 2**20),
        name="front",
    )(edge, rows, mods, gain, w_dt, taps, rate, extra, w_x, w_g, w_bc)


def last_kernel(parts, latent, gate, w_out, out, buf, sems):
    n, _, cols = parts.shape
    copies = [
        pltpu.make_async_copy(w_out.at[pl.ds(i * cols, cols)], buf.at[pl.ds(i * cols, cols)], sems.at[i])
        for i in range(n)
    ]
    for c in copies:
        c.start()
    acc = jnp.zeros(out.shape, F32)
    for i in range(n):
        copies[i].wait()
        acc = acc + jnp.dot(parts[i], buf[i * cols : (i + 1) * cols, :], preferred_element_type=F32)
    out[...] = (latent[...].astype(F32) + gate[...] * acc).astype(BF16)


def last(parts, latent, gate, w_out):
    vmem = pl.BlockSpec(memory_space=pltpu.VMEM)
    return pl.pallas_call(
        last_kernel,
        out_shape=jax.ShapeDtypeStruct(latent.shape, BF16),
        in_specs=[vmem, vmem, vmem, pl.BlockSpec(memory_space=pl.ANY)],
        out_specs=vmem,
        scratch_shapes=[pltpu.VMEM(w_out.shape, BF16), pltpu.SemaphoreType.DMA((parts.shape[0],))],
        compiler_params=pltpu.CompilerParams(vmem_limit_bytes=24 * 2**20),
        name="last",
    )(parts, latent, gate, w_out)


def entry_sums(states, totals, f_lane):
    n = states.shape[0]
    m = lax.broadcasted_iota(jnp.int32, (n + 1, n, n, 1), 0)
    k = lax.broadcasted_iota(jnp.int32, (n + 1, n, n, 1), 1)
    j = lax.broadcasted_iota(jnp.int32, (n + 1, n, n, 1), 2)
    mb = jnp.where(m == n, -1, m)
    between = jnp.where(f_lane, (j > k) & (j < m), (j < k) & (j > mb))
    gap = jnp.sum(jnp.where(between, totals[None, None], 0.0), axis=2)
    ahead = jnp.where(f_lane, k[:, :, 0] < m[:, :, 0], k[:, :, 0] > mb[:, :, 0])
    factor = jnp.where(ahead, jnp.exp(gap), 0.0)
    sums = jnp.sum(factor[:, :, None] * states[None], axis=1)
    to_m = jnp.sum(jnp.where(ahead, totals[None], 0.0), axis=1)
    return sums, to_m


def entry_states(near, heads):
    n = near.shape[0]
    half = heads * STATE // n
    near = exchange(near, NEAR).astype(F32)
    f_lane = lax.broadcasted_iota(jnp.int32, (1, 128), 1) < HEAD_DIM
    ctx_t = near[:, 2 * half] + near[:, 2 * half + 1]
    lat_t = near[:, 2 * half + 2] + near[:, 2 * half + 3]
    ctx_sums, ctx_to = entry_sums(near[:, :half], ctx_t, f_lane)
    lat_sums, lat_to = entry_sums(near[:, half : 2 * half], lat_t, f_lane)
    far = jnp.concatenate(
        [ctx_sums[n], lat_sums[n], *split_hi_lo(ctx_to[n:]), *split_hi_lo(lat_to[n:]), jnp.zeros((4, 128), F32)], axis=0
    ).astype(BF16)
    far = share(far, "za").astype(F32)
    count = far.shape[0]
    start, _ = entry_sums(far[:, :half], far[:, 2 * half] + far[:, 2 * half + 1], f_lane)
    group, group_to = entry_sums(far[:, half : 2 * half], far[:, 2 * half + 2] + far[:, 2 * half + 3], f_lane)
    mine = (jnp.arange(count + 1) == lax.axis_index("za")).astype(F32)
    group = jnp.sum(mine[:, None, None] * group, axis=0)
    group_to = jnp.sum(mine[:, None] * group_to, axis=0)
    entry = jnp.exp(group_to) * start[count] + group
    back = (jnp.exp(lat_to[:n, None]) * entry + lat_sums[:n]).astype(BF16)
    back = exchange(back, NEAR)
    return back.reshape(heads, STATE, 128)


def program(
    latent,
    cond,
    context,
    context_cond,
    modulation,
    norm_gain,
    w_x,
    w_gate,
    w_b,
    w_c,
    w_dt,
    conv_x,
    conv_b,
    conv_c,
    decay_rate,
    decay_extra,
    out_gain,
    w_out,
):
    heads = w_dt.shape[2]
    head_cols = w_x.shape[1]
    tokens = decay_extra.shape[0]
    count = lax.axis_size(SP)
    place = lax.axis_index(SP)
    up = [(i, i + 1) for i in range(count - 1)]
    down = [(i + 1, i) for i in range(count - 1)]
    low = lax.ppermute(jnp.concatenate([latent[-2:], context[-2:]]), SP, up)
    high = lax.ppermute(jnp.concatenate([latent[:1], context[:1]]), SP, down)

    def blank(n):
        return jnp.zeros((n, latent.shape[1]), BF16)

    own = jnp.concatenate([latent, low[:2], high[:1], blank(5)])
    mods, gathered = mod_vectors(cond, context_cond, modulation, own)
    tokens_own = latent.shape[0]
    rows = jnp.concatenate(
        [
            blank(PAD - 2),
            gathered[-1, tokens_own : tokens_own + 2],
            gathered[:, :tokens_own].reshape(tokens, latent.shape[1]),
            gathered[0, tokens_own + 2 : tokens_own + 3],
            blank(2 * PAD - 3),
            low[2:],
            context,
            high[1:],
            blank(PAD - 1),
        ]
    )
    near, xs, bc, z_act, running, dt, gate = front(
        jnp.stack([place == 0, place == count - 1]).astype(jnp.int32),
        rows,
        mods,
        norm_gain[None],
        jnp.concatenate([w_dt[0], w_dt[1]], axis=1).T,
        jnp.concatenate([conv_x, conv_b, conv_c], axis=1),
        decay_rate.reshape(1, 2 * heads),
        jnp.concatenate([decay_extra, decay_extra], axis=1),
        w_x,
        w_gate,
        jnp.concatenate([w_b, w_c], axis=1),
        lax.axis_size(NEAR),
    )
    bmat, cmat = bc[:, :STATE], bc[:, STATE:]
    entry = entry_states(near, heads)

    affinity = lax.dot_general(cmat, bmat, (((1,), (1,)), ((), ())), preferred_element_type=F32)
    i = jnp.arange(tokens)
    lower = i[:, None] >= i[None, :]
    upper = i[:, None] <= i[None, :]
    parts = []
    for h in range(heads):
        weights = jnp.zeros((tokens, tokens), F32)
        for d, mask in ((0, lower), (1, upper)):
            col = d * heads + h
            gap = running[:, col][:, None] - running[:, col][None, :]
            mixing = jnp.where(mask, jnp.exp(jnp.where(mask, gap, 0.0)), 0.0)
            weights = weights + mixing * dt[:, col][None, :]
        weights = (affinity * weights).astype(BF16)
        parts.append(jnp.dot(weights, xs[:, h * HEAD_DIM : (h + 1) * HEAD_DIM], preferred_element_type=F32))
    y = jnp.concatenate(parts, axis=1)
    flat = entry.transpose(1, 0, 2).reshape(STATE, heads * 128)
    carried = jnp.dot(cmat, flat, preferred_element_type=F32) * wide(jnp.exp(running))
    carried = carried.reshape(tokens, heads, 2, HEAD_DIM)
    y = y + (carried[:, :, 0] + carried[:, :, 1]).reshape(tokens, heads * HEAD_DIM)
    gated = y * z_act
    mean_square = jnp.mean(gated * gated, axis=1, keepdims=True)
    normed = (gated * lax.rsqrt(mean_square + GROUP_EPS) * out_gain.astype(F32)).astype(BF16)
    tp_count = lax.axis_size("tp")
    stacked = normed.reshape(tp_count, tokens // tp_count, head_cols)
    return last(exchange(stacked, "tp"), latent, gate, w_out)


def solution(mesh):
    sp, tp, dp = (mesh.shape[a] for a in ("sp", "tp", "dp"))
    inner = Mesh(np.asarray(mesh.devices).reshape(sp // 8, 4, 2, tp, dp), (*SP, "tp", "dp"))
    in_specs = (
        P(("dp", *SP, "tp"), None),
        P("dp"),
        P(("dp", *SP), None),
        P(),
        P((*SP, "tp"), None),
        P(),
        P(None, "tp"),
        P(None, "tp"),
        P(None, "tp"),
        P(None, "tp"),
        P(None, None, "tp"),
        P(None, "tp"),
        P(None, "tp"),
        P(None, "tp"),
        P(None, "tp"),
        P(("dp", *SP), "tp"),
        P("tp"),
        P(),
    )
    out_specs = P(("dp", *SP, "tp"), None)
    return jax.shard_map(program, mesh=inner, in_specs=in_specs, out_specs=out_specs, check_vma=False)
```

time: 178 us -> 194 us (1.090)
  the two profiles are of different devices: /device:TPU:4 before, /device:TPU:6 now
where the time goes in v3:
time: 194 us; the launch traced here: 192 us
  starting transfers between devices  71.9 us (37%)
  waiting for transfers between devices  62.4 us (32%)
  local copies, waits for them, and re-layouts  28.6 us (15%)
  blocking collectives  9.69 us (5%)
  other arithmetic  9.63 us (5%)
  Pallas kernels  7.77 us (4%)
    all_to_all x6, waiting for transfers between devices, exchange(): return lax.all_to_all(x, axis, 0, 0, tiled=True)  62.4 us
    all_to_all x6, starting transfers between devices, exchange(): return lax.all_to_all(x, axis, 0, 0, tiled=True)  55.4 us
    ppermute x3, starting transfers between devices, ring_rows(): lax.ppermute(x, 'tp', [(i, (i + k) % n) for i in range(n)])  11.3 us
    unnamed x58, local copies, waits for them, and re-layouts  10.7 us
    all_to_all x1, blocking collectives, exchange(): return lax.all_to_all(x, axis, 0, 0, tiled=True)  9.69 us
    pallas_call x1, Pallas kernels, front(): pl.pallas_call(front_kernel, out_shape=(shape((slots, 2 * half + 8, 128),...  4.66 us
    concatenate x1, local copies, waits for them, and re-layouts, program(): jnp.concatenate([blank(PAD - 2), gathered[-1, tokens_own:tokens_own + 2],...  4.44 us
    ppermute x1, starting transfers between devices, program(): low = lax.ppermute(jnp.concatenate([latent[-2:], context[-2:]]), SP, up)  3.93 us
  transfers between devices with their start and end apart: 11, of which 5 were waited for; matrix products, arithmetic and copies ran while one was open for 13% of the time, Pallas kernels for 0%

profile of v3, /device:TPU:6, one launch (start us, length us, event | category | flops | bytes accessed | tf_op | source)
XLA Modules:
  0.0 191.9 jit_solution(14487408470002256129)
XLA Ops:
  0.0 0.7 broadcast_in_dim.357.cond
  0.7 0.7 broadcast_in_dim.358.context_cond
  1.4 0.9 copy-done.6
  2.3 1.2 partial_mods.1
  3.5 5.8 %all-to-all-start = ((f32[40,2,128]{2,1,0:T(2,128)}), f32[40,2,128]{2,1,0:T(2,128)S(1)}, u32[]{:S(2)}, u32[]{:S(2)}) async-start(f32[40,2,128]{2,1,0:T(2,128)} %partial_mods.1), calls=%async_computation | async-start | bytes 81920 | tf_op jit(solution)/shard_map/all_to_all | solution.py:27
  9.4 0.8 slice.222
  10.1 0.8 slice.223
  10.9 3.9 %collective-permute-start = (bf16[4,2048]{1,0:T(4,128)(2,1)S(1)}, bf16[4,2048]{1,0:T(4,128)(2,1)S(1)}, u32[]{:S(2)}, u32[]{:S(2)}) collective-permute-start(bf16[4,2048]{1,0:T(4,128)(2,1)S(1)} %pad_maximum_fusion.5), channel_id=1, source_target_pairs={{0,32},{32,64},{64,96},{96,128},{128,160},{160,192},{192,224},{224... | collective-permute-start | bytes 49160 | tf_op jit(solution)/shard_map/ppermute | solution.py:361
  14.9 0.8 slice.225
  15.6 0.8 slice.226
  16.4 1.3 collective-permute-start.1
  18.3 0.7 slice_bitcast_fusion.1
  19.1 1.2 copy.110
  24.7 3.4 %collective-permute-start.2 = (bf16[40,2048]{1,0:T(8,128)(2,1)S(1)}, bf16[40,2048]{1,0:T(8,128)(2,1)S(1)}, u32[]{:S(2)}, u32[]{:S(2)}) collective-permute-start(bf16[40,2048]{1,0:T(8,128)(2,1)S(1)} %maximum_maximum_fusion), channel_id=1, source_target_pairs={{0,8},{8,16},{16,24},{24,0},{1,9},{9,17},{17,25},{25,1},{2,10},{10... | collective-permute-start | bytes 491528 | tf_op jit(solution)/shard_map/ppermute | solution.py:38
  28.1 4.6 %collective-permute-start.3 = (bf16[40,2048]{1,0:T(8,128)(2,1)S(1)}, bf16[40,2048]{1,0:T(8,128)(2,1)S(1)}, u32[]{:S(2)}, u32[]{:S(2)}) collective-permute-start(bf16[40,2048]{1,0:T(8,128)(2,1)S(1)} %maximum_maximum_fusion), channel_id=1, source_target_pairs={{0,16},{8,24},{16,0},{24,8},{1,17},{9,25},{17,1},{25,9},{2,18},{10... | collective-permute-start | bytes 491528 | tf_op jit(solution)/shard_map/ppermute | solution.py:38
  32.7 3.4 %collective-permute-start.4 = (bf16[40,2048]{1,0:T(8,128)(2,1)S(1)}, bf16[40,2048]{1,0:T(8,128)(2,1)S(1)}, u32[]{:S(2)}, u32[]{:S(2)}) collective-permute-start(bf16[40,2048]{1,0:T(8,128)(2,1)S(1)} %maximum_maximum_fusion), channel_id=1, source_target_pairs={{0,24},{8,0},{16,8},{24,16},{1,25},{9,1},{17,9},{25,17},{2,26},{10... | collective-permute-start | bytes 491528 | tf_op jit(solution)/shard_map/ppermute | solution.py:38
  36.6 0.7 copy.112.extra
  37.4 0.7 reshape.377.rate
  38.0 0.7 pad_maximum_fusion.8.taps
  38.7 0.7 broadcast_in_dim.362
  39.3 29.9 %all-to-all-start.1 = ((f32[80,2,128]{2,1,0:T(2,128)}), f32[80,2,128]{2,1,0:T(2,128)S(1)}, u32[]{:S(2)}, u32[]{:S(2)}) async-start(f32[80,2,128]{2,1,0:T(2,128)} %bitcast.11), calls=%async_computation.1 | async-start | bytes 163840 | tf_op jit(solution)/shard_map/all_to_all | solution.py:27
  69.5 22.9 %all-to-all-done.1 = f32[80,2,128]{2,1,0:T(2,128)S(1)} async-done(((f32[80,2,128]{2,1,0:T(2,128)}), f32[80,2,128]{2,1,0:T(2,128)S(1)}, u32[]{:S(2)}, u32[]{:S(2)}) %all-to-all-start.1) | async-done | bytes 81952 | tf_op jit(solution)/shard_map/all_to_all | solution.py:27
  93.1 3.3 %all-to-all-start.2 = ((f32[40,2,128]{2,1,0:T(2,128)}), f32[40,2,128]{2,1,0:T(2,128)S(1)}, u32[]{:S(2)}, u32[]{:S(2)}) async-start(f32[40,2,128]{2,1,0:T(2,128)} %bitcast.13), calls=%async_computation.2 | async-start | bytes 81920 | tf_op jit(solution)/shard_map/all_to_all | solution.py:27
  96.5 0.8 pad_maximum_fusion.1
  97.4 4.4 %concatenate.42.rows = bf16[176,2048]{1,0:T(8,128)(2,1)S(1)} concatenate(bf16[6,2048]{1,0:T(8,128)(2,1)S(1)} %broadcast_in_dim.356, bf16[2,2048]{1,0:T(2,128)(2,1)S(1)} %dynamic-slice_bitcast_fusion.1, bf16[128,2048]{1,0:T(8,128)(2,1)} %bitcast.68, bf16[1,2048]{1,0:T(2,128)(2,1)S(1)} %dynamic-slice_bitcast_fusion, bf16[13,2048]{1,0:T(8,128)(2,1)S(1)} %broadcast_in_dim.360, ...), dimensions={0} | concatenate | bytes 1441792 | tf_op jit(solution)/shard_map/concatenate | solution.py:370
  101.8 0.9 all-to-all-done.2.mods
  102.7 0.8 copy-done.5
  103.5 0.8 copy-done.8
  104.3 0.7 copy-done.11
  105.5 0.7 copy-done.15
  106.2 4.7 %front.1 = (bf16[8,72,128]{2,1,0:T(8,128)(2,1)S(1)}, bf16[128,256]{1,0:T(8,128)(2,1)S(1)}, bf16[128,128]{1,0:T(8,128)(2,1)S(1)}, f32[128,256]{1,0:T(8,128)S(1)},...) custom-call(s32[2]{0:T(128)S(1)} %copy-done.14, bf16[176,2048]{1,0:T(8,128)(2,1)S(1)} %concatenate.42.rows, ...), custom_call_target="tpu_custom_call" | custom-call | tf_op jit(solution)/shard_map/front/pallas_call | solution.py:240
  110.9 0.6 copy-done.7
  111.5 0.7 copy-done.9
  113.4 3.8 %all-to-all-start.3 = ((bf16[8,72,128]{2,1,0:T(8,128)(2,1)}), bf16[8,72,128]{2,1,0:T(8,128)(2,1)S(1)}, u32[]{:S(2)}, u32[]{:S(2)}) async-start(bf16[8,72,128]{2,1,0:T(8,128)(2,1)} %copy-done.7), calls=%async_computation.3 | async-start | bytes 294912 | tf_op jit(solution)/shard_map/all_to_all | solution.py:27
  117.3 0.7 copy.118
  118.0 0.7 copy.117
  118.7 0.8 copy.120
  119.6 0.7 convert_element_type.55
  120.3 0.7 fusion.51
  121.0 0.7 fusion.11
  122.5 6.4 %all-to-all-done.3 = bf16[8,72,128]{2,1,0:T(8,128)(2,1)S(1)} async-done(((bf16[8,72,128]{2,1,0:T(8,128)(2,1)}), bf16[8,72,128]{2,1,0:T(8,128)(2,1)S(1)}, u32[]{:S(2)}, u32[]{:S(2)}) %all-to-all-start.3) | async-done | bytes 147488 | tf_op jit(solution)/shard_map/all_to_all | solution.py:27
  130.3 8.3 %all-to-all-start.4 = ((bf16[4,72,128]{2,1,0:T(8,128)(2,1)}), bf16[4,72,128]{2,1,0:T(8,128)(2,1)S(1)}, u32[]{:S(2)}, u32[]{:S(2)}) async-start(bf16[4,72,128]{2,1,0:T(8,128)(2,1)} %broadcast_in_dim.385), calls=%async_computation.4 | async-start | bytes 147456 | tf_op jit(solution)/shard_map/all_to_all | solution.py:27
  138.8 22.3 %all-to-all-done.4 = bf16[4,72,128]{2,1,0:T(8,128)(2,1)S(1)} async-done(((bf16[4,72,128]{2,1,0:T(8,128)(2,1)}), bf16[4,72,128]{2,1,0:T(8,128)(2,1)S(1)}, u32[]{:S(2)}, u32[]{:S(2)}) %all-to-all-start.4) | async-done | bytes 73760 | tf_op jit(solution)/shard_map/all_to_all | solution.py:27
  162.3 4.1 %all-to-all-start.5 = ((bf16[8,32,128]{2,1,0:T(8,128)(2,1)}), bf16[8,32,128]{2,1,0:T(8,128)(2,1)S(1)}, u32[]{:S(2)}, u32[]{:S(2)}) async-start(bf16[8,32,128]{2,1,0:T(8,128)(2,1)} %fusion.2), calls=%async_computation.5 | async-start | bytes 131072 | tf_op jit(solution)/shard_map/all_to_all | solution.py:27
  167.4 9.9 %all-to-all-done.5 = bf16[8,32,128]{2,1,0:T(8,128)(2,1)S(1)} async-done(((bf16[8,32,128]{2,1,0:T(8,128)(2,1)}), bf16[8,32,128]{2,1,0:T(8,128)(2,1)S(1)}, u32[]{:S(2)}, u32[]{:S(2)}) %all-to-all-start.5) | async-done | bytes 65568 | tf_op jit(solution)/shard_map/all_to_all | solution.py:27
  178.1 9.7 %all_to_all.36.parts = bf16[4,32,256]{2,1,0:T(8,128)(2,1)S(1)} all-to-all(bf16[4,32,256]{2,1,0:T(8,128)(2,1)S(1)} %bitcast.75), channel_id=1, replica_groups=mesh['za'=4,'zb'=4,'zc'=2,'tp'=4,'dp'=8] {'tp'}, dimensions={0} | all-to-all | bytes 131072 | tf_op jit(solution)/shard_map/all_to_all | solution.py:27
  187.8 2.2 %copy-done = bf16[1024,2048]{1,0:T(8,128)(2,1)S(1)} copy-done((bf16[1024,2048]{1,0:T(8,128)(2,1)S(1)}, bf16[1024,2048]{1,0:T(8,128)(2,1)}, u32[]{:S(2)}) %copy-start) | copy-done | bytes 4194328
  190.0 1.9 last.1
  (130 shorter events, 13.6 us)
Async XLA Ops:
  0.0 20.6 %copy-start.21 = (f32[128,4]{0,1:T(4,128)S(1)}, f32[128,4]{0,1:T(4,128)}, u32[]{:S(2)}) copy-start(f32[128,4]{0,1:T(4,128)} %param.33) | copy-start | bytes 6148
  1.4 0.9 copy-start.6
  2.3 18.0 %copy-start.18 = (bf16[2048,64]{0,1:T(8,128)(2,1)S(1)}, bf16[2048,64]{0,1:T(8,128)(2,1)}, u32[]{:S(2)}) copy-start(bf16[2048,64]{0,1:T(8,128)(2,1)} %param.27) | copy-start | bytes 786436
  3.5 21.1 %all-to-all-start = ((f32[40,2,128]{2,1,0:T(2,128)}), f32[40,2,128]{2,1,0:T(2,128)S(1)}, u32[]{:S(2)}, u32[]{:S(2)}) async-start(f32[40,2,128]{2,1,0:T(2,128)} %partial_mods.1), calls=%async_computation | async-start | bytes 81920 | tf_op jit(solution)/shard_map/all_to_all | solution.py:27
  10.9 13.0 %collective-permute-start = (bf16[4,2048]{1,0:T(4,128)(2,1)S(1)}, bf16[4,2048]{1,0:T(4,128)(2,1)S(1)}, u32[]{:S(2)}, u32[]{:S(2)}) collective-permute-start(bf16[4,2048]{1,0:T(4,128)(2,1)S(1)} %pad_maximum_fusion.5), channel_id=1, source_target_pairs={{0,32},{32,64},{64,96},{96,128},{128,160},{160,192},{192,224},{224... | collective-permute-start | bytes 49160 | tf_op jit(solution)/shard_map/ppermute | solution.py:361
  16.4 6.9 %collective-permute-start.1 = (bf16[2,2048]{1,0:T(2,128)(2,1)S(1)}, bf16[2,2048]{1,0:T(2,128)(2,1)S(1)}, u32[]{:S(2)}, u32[]{:S(2)}) collective-permute-start(bf16[2,2048]{1,0:T(2,128)(2,1)S(1)} %pad_maximum_fusion.6), channel_id=1, source_target_pairs={{32,0},{64,32},{96,64},{128,96},{160,128},{192,160},{224,192},{256... | collective-permute-start | bytes 24584 | tf_op jit(solution)/shard_map/ppermute | solution.py:362
  17.8 4.1 %copy-start.25 = (pred[9]{0:T(512)(128)(4,1)}, pred[9]{0:T(512)(128)(4,1)S(1)}, u32[]{:S(2)}) copy-start(pred[9]{0:T(512)(128)(4,1)S(1)} %iota_compare_fusion.11) | copy-start | bytes 31
  18.3 3.5 %copy-start.26 = (pred[5]{0:T(512)(128)(4,1)}, pred[5]{0:T(512)(128)(4,1)S(1)}, u32[]{:S(2)}) copy-start(pred[5]{0:T(512)(128)(4,1)S(1)} %iota_compare_fusion.10) | copy-start | bytes 19
  20.3 4.2 %copy-start.3 = (bf16[32,2048]{1,0:T(8,128)(2,1)S(1)}, bf16[32,2048]{1,0:T(8,128)(2,1)}, u32[]{:S(2)}) copy-start(bf16[32,2048]{1,0:T(8,128)(2,1)} %latent.1) | copy-start | bytes 393220
  20.6 16.7 %copy-start.20 = (bf16[2048]{0:T(1024)(128)(2,1)S(1)}, bf16[2048]{0:T(1024)(128)(2,1)}, u32[]{:S(2)}) copy-start(bf16[2048]{0:T(1024)(128)(2,1)} %param.23) | copy-start | bytes 12292
  20.6 16.7 %copy-start.27 = (f32[2,4]{1,0:T(2,128)S(1)}, f32[2,4]{1,0:T(2,128)}, u32[]{:S(2)}) copy-start(f32[2,4]{1,0:T(2,128)} %param.32) | copy-start | bytes 100
  20.7 17.4 %copy-start.22 = (bf16[4,256]{1,0:T(4,128)(2,1)S(1)}, bf16[4,256]{1,0:T(4,128)(2,1)}, u32[]{:S(2)}) copy-start(bf16[4,256]{1,0:T(4,128)(2,1)} %param.29) | copy-start | bytes 6148
  20.7 17.4 %copy-start.23 = (bf16[4,64]{1,0:T(4,128)(2,1)S(1)}, bf16[4,64]{1,0:T(4,128)(2,1)}, u32[]{:S(2)}) copy-start(bf16[4,64]{1,0:T(4,128)(2,1)} %param.31) | copy-start | bytes 1540
  20.7 17.3 %copy-start.24 = (bf16[4,64]{1,0:T(4,128)(2,1)S(1)}, bf16[4,64]{1,0:T(4,128)(2,1)}, u32[]{:S(2)}) copy-start(bf16[4,64]{1,0:T(4,128)(2,1)} %param.30) | copy-start | bytes 1540
  24.7 44.6 %collective-permute-start.2 = (bf16[40,2048]{1,0:T(8,128)(2,1)S(1)}, bf16[40,2048]{1,0:T(8,128)(2,1)S(1)}, u32[]{:S(2)}, u32[]{:S(2)}) collective-permute-start(bf16[40,2048]{1,0:T(8,128)(2,1)S(1)} %maximum_maximum_fusion), channel_id=1, source_target_pairs={{0,8},{8,16},{16,24},{24,0},{1,9},{9,17},{17,25},{25,1},{2,10},{10... | collective-permute-start | bytes 491528 | tf_op jit(solution)/shard_map/ppermute | solution.py:38
  28.1 41.2 %collective-permute-start.3 = (bf16[40,2048]{1,0:T(8,128)(2,1)S(1)}, bf16[40,2048]{1,0:T(8,128)(2,1)S(1)}, u32[]{:S(2)}, u32[]{:S(2)}) collective-permute-start(bf16[40,2048]{1,0:T(8,128)(2,1)S(1)} %maximum_maximum_fusion), channel_id=1, source_target_pairs={{0,16},{8,24},{16,0},{24,8},{1,17},{9,25},{17,1},{25,9},{2,18},{10... | collective-permute-start | bytes 491528 | tf_op jit(solution)/shard_map/ppermute | solution.py:38
  32.7 36.6 %collective-permute-start.4 = (bf16[40,2048]{1,0:T(8,128)(2,1)S(1)}, bf16[40,2048]{1,0:T(8,128)(2,1)S(1)}, u32[]{:S(2)}, u32[]{:S(2)}) collective-permute-start(bf16[40,2048]{1,0:T(8,128)(2,1)S(1)} %maximum_maximum_fusion), channel_id=1, source_target_pairs={{0,24},{8,0},{16,8},{24,16},{1,25},{9,1},{17,9},{25,17},{2,26},{10... | collective-permute-start | bytes 491528 | tf_op jit(solution)/shard_map/ppermute | solution.py:38
  39.3 53.1 %all-to-all-start.1 = ((f32[80,2,128]{2,1,0:T(2,128)}), f32[80,2,128]{2,1,0:T(2,128)S(1)}, u32[]{:S(2)}, u32[]{:S(2)}) async-start(f32[80,2,128]{2,1,0:T(2,128)} %bitcast.11), calls=%async_computation.1 | async-start | bytes 163840 | tf_op jit(solution)/shard_map/all_to_all | solution.py:27
  93.1 9.6 %all-to-all-start.2 = ((f32[40,2,128]{2,1,0:T(2,128)}), f32[40,2,128]{2,1,0:T(2,128)S(1)}, u32[]{:S(2)}, u32[]{:S(2)}) async-start(f32[40,2,128]{2,1,0:T(2,128)} %bitcast.13), calls=%async_computation.2 | async-start | bytes 81920 | tf_op jit(solution)/shard_map/all_to_all | solution.py:27
  96.5 6.2 %copy-start.1 = (bf16[2048,256]{1,0:T(8,128)(2,1)S(1)}, bf16[2048,256]{1,0:T(8,128)(2,1)}, u32[]{:S(2)}) copy-start(bf16[2048,256]{1,0:T(8,128)(2,1)} %w_x.1) | copy-start | bytes 3145732
  96.5 6.2 %copy-start.2 = (bf16[2048,256]{1,0:T(8,128)(2,1)S(1)}, bf16[2048,256]{1,0:T(8,128)(2,1)}, u32[]{:S(2)}) copy-start(bf16[2048,256]{1,0:T(8,128)(2,1)} %w_g.1) | copy-start | bytes 3145732
  102.7 0.8 copy-start.5
  103.5 0.8 copy-start.8
  104.3 0.7 copy-start.11
  105.0 0.6 copy-start.14
  105.5 0.7 copy-start.15
  110.9 0.7 copy-start.7
  111.5 0.7 copy-start.9
  112.2 0.6 copy-start.12
  112.8 0.6 copy-start.16
  113.4 15.5 %copy-start.19 = (pred[128]{0:T(512)(128)(4,1)S(1)}, pred[128]{0:T(512)(128)(4,1)}, u32[]{:S(2)}) copy-start(pred[128]{0:T(512)(128)(4,1)} %iota_compare_fusion.12) | copy-start | bytes 388
  113.4 15.5 %all-to-all-start.3 = ((bf16[8,72,128]{2,1,0:T(8,128)(2,1)}), bf16[8,72,128]{2,1,0:T(8,128)(2,1)S(1)}, u32[]{:S(2)}, u32[]{:S(2)}) async-start(bf16[8,72,128]{2,1,0:T(8,128)(2,1)} %copy-done.7), calls=%async_computation.3 | async-start | bytes 294912 | tf_op jit(solution)/shard_map/all_to_all | solution.py:27
  122.3 16.3 %copy-start.17 = (bf16[128,256]{1,0:T(8,128)(2,1)S(1)}, bf16[128,256]{1,0:T(8,128)(2,1)}, u32[]{:S(2)}) copy-start(bf16[128,256]{1,0:T(8,128)(2,1)} %copy-done.16) | copy-start | bytes 196612
  130.3 30.8 %all-to-all-start.4 = ((bf16[4,72,128]{2,1,0:T(8,128)(2,1)}), bf16[4,72,128]{2,1,0:T(8,128)(2,1)S(1)}, u32[]{:S(2)}, u32[]{:S(2)}) async-start(bf16[4,72,128]{2,1,0:T(8,128)(2,1)} %broadcast_in_dim.385), calls=%async_computation.4 | async-start | bytes 147456 | tf_op jit(solution)/shard_map/all_to_all | solution.py:27
  162.3 15.0 %all-to-all-start.5 = ((bf16[8,32,128]{2,1,0:T(8,128)(2,1)}), bf16[8,32,128]{2,1,0:T(8,128)(2,1)S(1)}, u32[]{:S(2)}, u32[]{:S(2)}) async-start(bf16[8,32,128]{2,1,0:T(8,128)(2,1)} %fusion.2), calls=%async_computation.5 | async-start | bytes 131072 | tf_op jit(solution)/shard_map/all_to_all | solution.py:27
  166.9 10.9 %copy-start.10 = (f32[128,256]{1,0:T(8,128)S(1)}, f32[128,256]{1,0:T(8,128)}, u32[]{:S(2)}) copy-start(f32[128,256]{1,0:T(8,128)} %copy-done.9) | copy-start | bytes 393220
  177.5 10.3 %copy-start.4 = (bf16[32,2048]{1,0:T(8,128)(2,1)S(1)}, bf16[32,2048]{1,0:T(8,128)(2,1)}, u32[]{:S(2)}) copy-start(bf16[32,2048]{1,0:T(8,128)(2,1)} %latent.1) | copy-start | bytes 393220
  177.5 10.3 %copy-start.13 = (f32[1,2048]{1,0:T(1,128)S(1)}, f32[1,2048]{1,0:T(1,128)}, u32[]{:S(2)}) copy-start(f32[1,2048]{1,0:T(1,128)} %copy-done.12) | copy-start | bytes 24580
  187.8 2.2 %copy-start = (bf16[1024,2048]{1,0:T(8,128)(2,1)S(1)}, bf16[1024,2048]{1,0:T(8,128)(2,1)}, u32[]{:S(2)}) copy-start(bf16[1024,2048]{1,0:T(8,128)(2,1)} %w_out.1) | copy-start | bytes 12582916

commit v4 on v2

--- a/solution.py
+++ b/solution.py
@@ -2,6 +2,8 @@
 import jax.numpy as jnp
 import numpy as np
 from jax import lax
+from jax.experimental import pallas as pl
+from jax.experimental.pallas import tpu as pltpu
 from jax.sharding import Mesh
 from jax.sharding import PartitionSpec as P
 
@@ -44,18 +46,53 @@
     return hi, x - hi
 
 
+def whole(shape):
+    return pl.BlockSpec(shape, lambda i: (0,) * len(shape))
+
+
+def silu(v):
+    return v / (1.0 + jnp.exp(-v))
+
+
+def partial_kernel(first, cond, context_cond, modulation, out):
+    share_rows, cols = modulation.shape
+    width = cols // 3
+    at = first[0] + lax.broadcasted_iota(jnp.int32, (share_rows, width), 0)
+    pick = jnp.where(lax.broadcasted_iota(jnp.int32, (share_rows, width), 1) == at, 1.0, 0.0).astype(BF16)
+    table = modulation[...]
+    cut = width // (out.shape[0] // 5)
+    for source, kinds in ((0, (0, 1, 2)), (1, (0, 1))):
+        v = (cond, context_cond)[source][...].astype(F32).reshape(1, width)
+        row = silu(v).astype(BF16)
+        own = lax.dot_general(row, pick, (((1,), (1,)), ((), ())), preferred_element_type=F32).astype(BF16)
+        sums = jnp.dot(own, table, preferred_element_type=F32)
+        for kind in kinds:
+            for n in range(width // cut):
+                for r in range(2):
+                    at = kind * width + n * cut + r * 128
+                    out[n * 5 + 3 * source + kind, r : r + 1, :] = sums[0:1, at : at + 128]
+
+
+def partial_mods(first, cond, context_cond, modulation, n):
+    return pl.pallas_call(
+        partial_kernel,
+        grid=(1,),
+        out_shape=jax.ShapeDtypeStruct((n * 5, 2, 128), F32),
+        in_specs=[pl.BlockSpec(memory_space=pltpu.SMEM)] + [whole(v.shape) for v in (cond, context_cond, modulation)],
+        out_specs=whole((n * 5, 2, 128)),
+        name="partial_mods",
+    )(first.astype(jnp.int32).reshape(1), cond, context_cond, modulation)
+
+
 def mod_vectors(cond, context_cond, modulation, own_rows):
     share_rows = modulation.shape[0]
     width = modulation.shape[1] // 3
-    rows = jax.nn.silu(jnp.stack([cond, context_cond]).astype(F32)).astype(BF16)
-    own = lax.dynamic_slice_in_dim(rows, lax.axis_index((*SP, "tp")) * share_rows, share_rows, 1)
-    part = jnp.dot(own, modulation, preferred_element_type=F32)
     n = lax.axis_size(MOD_NEAR)
     cut = width // n
     pairs = 5 * cut // 256
-    part = part.reshape(6, n, cut)[:5].transpose(1, 0, 2).reshape(n * pairs, 2, 128)
+    first = lax.axis_index((*SP, "tp")) * share_rows
+    part = partial_mods(first, cond, context_cond, modulation, n)
     part = jnp.sum(exchange(part, MOD_NEAR).reshape(n, pairs, 2, 128), axis=0)
-    part, own_rows = lax.optimization_barrier((part, own_rows))
     far = share(part, MOD_FAR)
     gathered = ring_rows(own_rows)
     full = share(jnp.sum(far, axis=0), MOD_NEAR)
@@ -186,6 +223,7 @@
     low = lax.ppermute(jnp.concatenate([latent[-PAD:], context[-PAD:]]), SP, up)
     high = lax.ppermute(jnp.concatenate([latent[:PAD], context[:PAD]]), SP, down)
     own = jnp.concatenate([latent, low[:PAD], high[:PAD]])
+    context_rows = jnp.concatenate([low[PAD:], context, high[PAD:]])
     mods, gathered = mod_vectors(cond, context_cond, modulation, own)
     tokens_own = latent.shape[0]
     latent_rows = jnp.concatenate(
@@ -195,7 +233,6 @@
             gathered[0, tokens_own + PAD :],
         ]
     )
-    context_rows = jnp.concatenate([low[PAD:], context, high[PAD:]])
 
     lat_len = tokens + 2 * PAD
     hidden = jnp.concatenate(

time: 178 us -> 181 us (1.017)
  the two profiles are of different devices: /device:TPU:4 before, /device:TPU:2 now
where the time goes in v4:
time: 181 us; the launch traced here: 180 us
  waiting for transfers between devices  73.3 us (40%)
  starting transfers between devices  70.1 us (39%)
  matrix products  8.83 us (5%)
  other arithmetic  8.69 us (5%)
  local copies, waits for them, and re-layouts  7.99 us (4%)
  blocking collectives  7.99 us (4%)
  Pallas kernels  2.28 us (1%)
    all_to_all x6, waiting for transfers between devices, exchange(): return lax.all_to_all(x, axis, 0, 0, tiled=True)  73.3 us
    all_to_all x6, starting transfers between devices, exchange(): return lax.all_to_all(x, axis, 0, 0, tiled=True)  53.5 us
    ppermute x3, starting transfers between devices, ring_rows(): lax.ppermute(x, 'tp', [(i, (i + k) % n) for i in range(n)])  10.7 us
    all_to_all x1, blocking collectives, program(): lax.all_to_all(stacked, 'tp', split_axis=0, concat_axis=2, tiled=True)[0]  7.99 us
    ppermute x1, starting transfers between devices, program(): low = lax.ppermute(jnp.concatenate([latent[-PAD:], context[-PAD:]]), SP, up)  4.56 us
    dot_general x1, matrix products, program(): branch = jnp.dot(full, w_out, preferred_element_type=F32)  3.68 us
  transfers between devices with their start and end apart: 11, of which 5 were waited for; matrix products, arithmetic and copies ran while one was open for 5% of the time, Pallas kernels for 0%

profile of v4, /device:TPU:2, one launch (start us, length us, event | category | flops | bytes accessed | tf_op | source)
XLA Modules:
  0.0 179.9 jit_solution(10787301667735575430)
XLA Ops:
  0.0 2.3 %partial_mods.1 = f32[40,2,128]{2,1,0:T(2,128)} custom-call(s32[1]{0:T(128)} %bitcast.first, bf16[2048]{0:T(1024)(128)(2,1)} %cond.1, bf16[2048]{0:T(1024)(128)(2,1)} %context_cond.1, bf16[16,6144]{1,0:T(8,128)(2,1)} %modulation.1), custom_call_target="tpu_custom_call" | custom-call | tf_op jit(solution)/shard_map/partial_mods/pallas_call | solution.py:77
  2.3 5.8 %all-to-all-start = ((f32[40,2,128]{2,1,0:T(2,128)}), f32[40,2,128]{2,1,0:T(2,128)S(1)}, u32[]{:S(2)}, u32[]{:S(2)}) async-start(f32[40,2,128]{2,1,0:T(2,128)} %partial_mods.1), calls=%async_computation | async-start | bytes 81920 | tf_op jit(solution)/shard_map/all_to_all | solution.py:27
  8.1 0.8 fusion.141
  9.0 1.3 collective-permute-start.1
  10.3 4.6 %collective-permute-start = (bf16[16,2048]{1,0:T(8,128)(2,1)S(1)}, bf16[16,2048]{1,0:T(8,128)(2,1)S(1)}, u32[]{:S(2)}, u32[]{:S(2)}) collective-permute-start(bf16[16,2048]{1,0:T(8,128)(2,1)S(1)} %pad_maximum_fusion.11), channel_id=1, source_target_pairs={{0,32},{32,64},{64,96},{96,128},{128,160},{160,192},{192,224},{224... | collective-permute-start | bytes 196616 | tf_op jit(solution)/shard_map/ppermute | solution.py:223
  15.2 0.7 convert_element_type.175
  15.9 0.7 slice_bitcast_fusion.1
  16.6 0.7 neg.40
  17.4 0.8 bitcast_convert_fusion.3
  18.2 0.8 bitcast_convert_fusion.7
  19.1 0.8 slice_convert_fusion.5
  20.3 0.7 convert_element_type.210
  21.1 5.1 %collective-permute-start.4 = (bf16[48,2048]{1,0:T(8,128)(2,1)S(1)}, bf16[48,2048]{1,0:T(8,128)(2,1)S(1)}, u32[]{:S(2)}, u32[]{:S(2)}) collective-permute-start(bf16[48,2048]{1,0:T(8,128)(2,1)S(1)} %get-tuple-element.24), channel_id=1, source_target_pairs={{0,24},{8,0},{16,8},{24,16},{1,25},{9,1},{17,9},{25,17},{2,26},{10... | collective-permute-start | bytes 589832 | tf_op jit(solution)/shard_map/ppermute | solution.py:38
  26.2 2.8 %collective-permute-start.3 = (bf16[48,2048]{1,0:T(8,128)(2,1)S(1)}, bf16[48,2048]{1,0:T(8,128)(2,1)S(1)}, u32[]{:S(2)}, u32[]{:S(2)}) collective-permute-start(bf16[48,2048]{1,0:T(8,128)(2,1)S(1)} %get-tuple-element.24), channel_id=1, source_target_pairs={{0,16},{8,24},{16,0},{24,8},{1,17},{9,25},{17,1},{25,9},{2,18},{10... | collective-permute-start | bytes 589832 | tf_op jit(solution)/shard_map/ppermute | solution.py:38
  29.0 2.8 %collective-permute-start.2 = (bf16[48,2048]{1,0:T(8,128)(2,1)S(1)}, bf16[48,2048]{1,0:T(8,128)(2,1)S(1)}, u32[]{:S(2)}, u32[]{:S(2)}) collective-permute-start(bf16[48,2048]{1,0:T(8,128)(2,1)S(1)} %get-tuple-element.24), channel_id=1, source_target_pairs={{0,8},{8,16},{16,24},{24,0},{1,9},{9,17},{17,25},{25,1},{2,10},{10... | collective-permute-start | bytes 589832 | tf_op jit(solution)/shard_map/ppermute | solution.py:38
  31.9 0.7 broadcast_in_dim.439
  32.6 27.5 %all-to-all-start.1 = ((f32[80,2,128]{2,1,0:T(2,128)}), f32[80,2,128]{2,1,0:T(2,128)S(1)}, u32[]{:S(2)}, u32[]{:S(2)}) async-start(f32[80,2,128]{2,1,0:T(2,128)} %bitcast.2), calls=%async_computation.1 | async-start | bytes 163840 | tf_op jit(solution)/shard_map/all_to_all | solution.py:27
  60.4 23.2 %all-to-all-done.1 = f32[80,2,128]{2,1,0:T(2,128)S(1)} async-done(((f32[80,2,128]{2,1,0:T(2,128)}), f32[80,2,128]{2,1,0:T(2,128)S(1)}, u32[]{:S(2)}, u32[]{:S(2)}) %all-to-all-start.1) | async-done | bytes 81952 | tf_op jit(solution)/shard_map/all_to_all | solution.py:27
  83.7 0.6 broadcast_in_dim.440
  84.3 4.9 %all-to-all-start.2 = ((f32[40,2,128]{2,1,0:T(2,128)}), f32[40,2,128]{2,1,0:T(2,128)S(1)}, u32[]{:S(2)}, u32[]{:S(2)}) async-start(f32[40,2,128]{2,1,0:T(2,128)} %bitcast.4), calls=%async_computation.2 | async-start | bytes 81920 | tf_op jit(solution)/shard_map/all_to_all | solution.py:27
  89.2 0.2 fusion.2
  89.4 6.1 %all-to-all-done.2 = f32[40,2,128]{2,1,0:T(2,128)S(1)} async-done(((f32[40,2,128]{2,1,0:T(2,128)}), f32[40,2,128]{2,1,0:T(2,128)S(1)}, u32[]{:S(2)}, u32[]{:S(2)}) %all-to-all-start.2) | async-done | bytes 40992 | tf_op jit(solution)/shard_map/all_to_all | solution.py:27
  95.6 0.3 fusion.6
  96.0 0.3 compare_select_fusion
  96.3 0.2 fusion.138
  96.8 0.2 fusion.139
  97.3 0.3 fusion.11
  97.8 0.4 fusion.8
  99.0 0.2 fusion.13
  100.4 1.9 %concatenate.67 = bf16[8,72,128]{2,1,0:T(8,128)(2,1)} concatenate(bf16[8,32,128]{2,1,0:T(8,128)(2,1)S(1)} %bitcast.211, bf16[8,32,128]{2,1,0:T(8,128)(2,1)S(1)} %bitcast.212, bf16[8,1,128]{2,1,0:T(2,128)(2,1)S(1)} %copy.209, bf16[8,1,128]{2,1,0:T(2,128)(2,1)S(1)} %copy.210, bf16[8,1,128]{2,1,0:T(2,128)(2,1)S(1)} %copy.211, bf16[8,1,128]{2,1,0:T(2,128)(2,1)S(1)} %copy.212, ...), dimensions={1} | concatenate | bytes 294912 | tf_op jit(solution)/shard_map/concatenate | solution.py:172
  102.4 3.4 %all-to-all-start.3 = ((bf16[8,72,128]{2,1,0:T(8,128)(2,1)}), bf16[8,72,128]{2,1,0:T(8,128)(2,1)S(1)}, u32[]{:S(2)}, u32[]{:S(2)}) async-start(bf16[8,72,128]{2,1,0:T(8,128)(2,1)} %concatenate.67), calls=%async_computation.3 | async-start | bytes 294912 | tf_op jit(solution)/shard_map/all_to_all | solution.py:27
  105.8 0.3 fusion.15
  106.1 0.2 fusion.147
  106.3 0.2 fusion.48
  106.6 10.8 %all-to-all-done.3 = bf16[8,72,128]{2,1,0:T(8,128)(2,1)S(1)} async-done(((bf16[8,72,128]{2,1,0:T(8,128)(2,1)}), bf16[8,72,128]{2,1,0:T(8,128)(2,1)S(1)}, u32[]{:S(2)}, u32[]{:S(2)}) %all-to-all-start.3) | async-done | bytes 147488 | tf_op jit(solution)/shard_map/all_to_all | solution.py:27
  117.4 0.3 fusion.18
  118.1 0.6 broadcast_in_dim.480
  118.7 8.5 %all-to-all-start.4 = ((bf16[4,72,128]{2,1,0:T(8,128)(2,1)}), bf16[4,72,128]{2,1,0:T(8,128)(2,1)S(1)}, u32[]{:S(2)}, u32[]{:S(2)}) async-start(bf16[4,72,128]{2,1,0:T(8,128)(2,1)} %broadcast_in_dim.480), calls=%async_computation.4 | async-start | bytes 147456 | tf_op jit(solution)/shard_map/all_to_all | solution.py:27
  127.3 0.2 fusion.50
  127.5 23.0 %all-to-all-done.4 = bf16[4,72,128]{2,1,0:T(8,128)(2,1)S(1)} async-done(((bf16[4,72,128]{2,1,0:T(8,128)(2,1)}), bf16[4,72,128]{2,1,0:T(8,128)(2,1)S(1)}, u32[]{:S(2)}, u32[]{:S(2)}) %all-to-all-start.4) | async-done | bytes 73760 | tf_op jit(solution)/shard_map/all_to_all | solution.py:27
  151.1 0.6 fusion.25
  151.7 3.4 %all-to-all-start.5 = ((bf16[8,32,128]{2,1,0:T(8,128)(2,1)}), bf16[8,32,128]{2,1,0:T(8,128)(2,1)S(1)}, u32[]{:S(2)}, u32[]{:S(2)}) async-start(bf16[8,32,128]{2,1,0:T(8,128)(2,1)} %fusion.25), calls=%async_computation.5 | async-start | bytes 131072 | tf_op jit(solution)/shard_map/all_to_all | solution.py:27
  155.3 0.2 fusion.52
  155.5 0.2 fusion.54
  155.7 10.2 %all-to-all-done.5 = bf16[8,32,128]{2,1,0:T(8,128)(2,1)S(1)} async-done(((bf16[8,32,128]{2,1,0:T(8,128)(2,1)}), bf16[8,32,128]{2,1,0:T(8,128)(2,1)S(1)}, u32[]{:S(2)}, u32[]{:S(2)}) %all-to-all-start.5) | async-done | bytes 65568 | tf_op jit(solution)/shard_map/all_to_all | solution.py:27
  166.4 1.6 multiply_reduce_fusion.4
  168.2 8.0 %all_to_all.46 = bf16[4,32,256]{2,1,0:T(8,128)(2,1)S(1)} all-to-all(bf16[4,32,256]{2,1,0:T(8,128)(2,1)S(1)} %bitcast.214), channel_id=1, replica_groups=mesh['za'=4,'zb'=4,'zc'=2,'tp'=4,'dp'=8] {'tp'}, dimensions={0} | all-to-all | bytes 131072 | tf_op jit(solution)/shard_map/all_to_all | solution.py:305
  176.2 3.7 %fusion.1 = bf16[32,2048]{1,0:T(8,128)(2,1)} fusion(bf16[32,1024]{1,0:T(8,128)(2,1)S(1)} %bitcast.210, bf16[1024,2048]{1,0:T(8,128)(2,1)} %param.35, bf16[32,2048]{1,0:T(8,128)(2,1)S(1)} %copy-done.1, f32[2048]{0:T(1024)S(1)} %bitcast.227), kind=kOutput, calls=%fused_computation.2 | convolution fusion | flops 134479872 | bytes 4530176 | tf_op jit(solution)/shard_map/dot_general | solution.py:306
  (130 shorter events, 5.8 us)
Async XLA Ops:
  0.0 97.7 %copy-start = (bf16[2048,256]{1,0:T(8,128)(2,1)S(1)}, bf16[2048,256]{1,0:T(8,128)(2,1)}, u32[]{:S(2)}) copy-start(bf16[2048,256]{1,0:T(8,128)(2,1)} %param.24) | copy-start | bytes 3145732
  0.0 21.0 %copy-start.1 = (bf16[32,2048]{1,0:T(8,128)(2,1)S(1)}, bf16[32,2048]{1,0:T(8,128)(2,1)}, u32[]{:S(2)}) copy-start(bf16[32,2048]{1,0:T(8,128)(2,1)} %param.18) | copy-start | bytes 393220
  0.0 31.7 %copy-start.2 = (bf16[16,2048]{1,0:T(8,128)(2,1)S(1)}, bf16[16,2048]{1,0:T(8,128)(2,1)}, u32[]{:S(2)}) copy-start(bf16[16,2048]{1,0:T(8,128)(2,1)} %param.20) | copy-start | bytes 196612
  2.3 29.6 %all-to-all-start = ((f32[40,2,128]{2,1,0:T(2,128)}), f32[40,2,128]{2,1,0:T(2,128)S(1)}, u32[]{:S(2)}, u32[]{:S(2)}) async-start(f32[40,2,128]{2,1,0:T(2,128)} %partial_mods.1), calls=%async_computation | async-start | bytes 81920 | tf_op jit(solution)/shard_map/all_to_all | solution.py:27
  9.0 12.0 %collective-permute-start.1 = (bf16[16,2048]{1,0:T(8,128)(2,1)S(1)}, bf16[16,2048]{1,0:T(8,128)(2,1)S(1)}, u32[]{:S(2)}, u32[]{:S(2)}) collective-permute-start(bf16[16,2048]{1,0:T(8,128)(2,1)S(1)} %pad_maximum_fusion.12), channel_id=1, source_target_pairs={{32,0},{64,32},{96,64},{128,96},{160,128},{192,160},{224,192},{256... | collective-permute-start | bytes 196616 | tf_op jit(solution)/shard_map/ppermute | solution.py:224
  10.3 10.7 %collective-permute-start = (bf16[16,2048]{1,0:T(8,128)(2,1)S(1)}, bf16[16,2048]{1,0:T(8,128)(2,1)S(1)}, u32[]{:S(2)}, u32[]{:S(2)}) collective-permute-start(bf16[16,2048]{1,0:T(8,128)(2,1)S(1)} %pad_maximum_fusion.11), channel_id=1, source_target_pairs={{0,32},{32,64},{64,96},{96,128},{128,160},{160,192},{192,224},{224... | collective-permute-start | bytes 196616 | tf_op jit(solution)/shard_map/ppermute | solution.py:223
  21.1 39.1 %collective-permute-start.4 = (bf16[48,2048]{1,0:T(8,128)(2,1)S(1)}, bf16[48,2048]{1,0:T(8,128)(2,1)S(1)}, u32[]{:S(2)}, u32[]{:S(2)}) collective-permute-start(bf16[48,2048]{1,0:T(8,128)(2,1)S(1)} %get-tuple-element.24), channel_id=1, source_target_pairs={{0,24},{8,0},{16,8},{24,16},{1,25},{9,1},{17,9},{25,17},{2,26},{10... | collective-permute-start | bytes 589832 | tf_op jit(solution)/shard_map/ppermute | solution.py:38
  26.2 34.0 %collective-permute-start.3 = (bf16[48,2048]{1,0:T(8,128)(2,1)S(1)}, bf16[48,2048]{1,0:T(8,128)(2,1)S(1)}, u32[]{:S(2)}, u32[]{:S(2)}) collective-permute-start(bf16[48,2048]{1,0:T(8,128)(2,1)S(1)} %get-tuple-element.24), channel_id=1, source_target_pairs={{0,16},{8,24},{16,0},{24,8},{1,17},{9,25},{17,1},{25,9},{2,18},{10... | collective-permute-start | bytes 589832 | tf_op jit(solution)/shard_map/ppermute | solution.py:38
  29.0 31.2 %collective-permute-start.2 = (bf16[48,2048]{1,0:T(8,128)(2,1)S(1)}, bf16[48,2048]{1,0:T(8,128)(2,1)S(1)}, u32[]{:S(2)}, u32[]{:S(2)}) collective-permute-start(bf16[48,2048]{1,0:T(8,128)(2,1)S(1)} %get-tuple-element.24), channel_id=1, source_target_pairs={{0,8},{8,16},{16,24},{24,0},{1,9},{9,17},{17,25},{25,1},{2,10},{10... | collective-permute-start | bytes 589832 | tf_op jit(solution)/shard_map/ppermute | solution.py:38
  32.6 51.0 %all-to-all-start.1 = ((f32[80,2,128]{2,1,0:T(2,128)}), f32[80,2,128]{2,1,0:T(2,128)S(1)}, u32[]{:S(2)}, u32[]{:S(2)}) async-start(f32[80,2,128]{2,1,0:T(2,128)} %bitcast.2), calls=%async_computation.1 | async-start | bytes 163840 | tf_op jit(solution)/shard_map/all_to_all | solution.py:27
  84.3 11.2 %all-to-all-start.2 = ((f32[40,2,128]{2,1,0:T(2,128)}), f32[40,2,128]{2,1,0:T(2,128)S(1)}, u32[]{:S(2)}, u32[]{:S(2)}) async-start(f32[40,2,128]{2,1,0:T(2,128)} %bitcast.4), calls=%async_computation.2 | async-start | bytes 81920 | tf_op jit(solution)/shard_map/all_to_all | solution.py:27
  95.5 0.8 copy-start.4
  95.6 1.7 copy-start.5
  98.3 7.5 %copy-start.3 = (bf16[2048,64]{0,1:T(8,128)(2,1)S(1)}, bf16[2048,64]{0,1:T(8,128)(2,1)}, u32[]{:S(2)}) copy-start(bf16[2048,64]{0,1:T(8,128)(2,1)} %param.27) | copy-start | bytes 786436
  102.4 15.0 %all-to-all-start.3 = ((bf16[8,72,128]{2,1,0:T(8,128)(2,1)}), bf16[8,72,128]{2,1,0:T(8,128)(2,1)S(1)}, u32[]{:S(2)}, u32[]{:S(2)}) async-start(bf16[8,72,128]{2,1,0:T(8,128)(2,1)} %concatenate.67), calls=%async_computation.3 | async-start | bytes 294912 | tf_op jit(solution)/shard_map/all_to_all | solution.py:27
  118.7 31.8 %all-to-all-start.4 = ((bf16[4,72,128]{2,1,0:T(8,128)(2,1)}), bf16[4,72,128]{2,1,0:T(8,128)(2,1)S(1)}, u32[]{:S(2)}, u32[]{:S(2)}) async-start(bf16[4,72,128]{2,1,0:T(8,128)(2,1)} %broadcast_in_dim.480), calls=%async_computation.4 | async-start | bytes 147456 | tf_op jit(solution)/shard_map/all_to_all | solution.py:27
  151.7 14.3 %all-to-all-start.5 = ((bf16[8,32,128]{2,1,0:T(8,128)(2,1)}), bf16[8,32,128]{2,1,0:T(8,128)(2,1)S(1)}, u32[]{:S(2)}, u32[]{:S(2)}) async-start(bf16[8,32,128]{2,1,0:T(8,128)(2,1)} %fusion.25), calls=%async_computation.5 | async-start | bytes 131072 | tf_op jit(solution)/shard_map/all_to_all | solution.py:27

commit v5 on v4

--- a/solution.py
+++ b/solution.py
@@ -84,7 +84,7 @@
     )(first.astype(jnp.int32).reshape(1), cond, context_cond, modulation)
 
 
-def mod_vectors(cond, context_cond, modulation, own_rows):
+def mod_vectors(cond, context_cond, modulation, own_rows, held):
     share_rows = modulation.shape[0]
     width = modulation.shape[1] // 3
     n = lax.axis_size(MOD_NEAR)
@@ -93,10 +93,11 @@
     first = lax.axis_index((*SP, "tp")) * share_rows
     part = partial_mods(first, cond, context_cond, modulation, n)
     part = jnp.sum(exchange(part, MOD_NEAR).reshape(n, pairs, 2, 128), axis=0)
+    part, held = lax.optimization_barrier((part, held))
     far = share(part, MOD_FAR)
     gathered = ring_rows(own_rows)
     full = share(jnp.sum(far, axis=0), MOD_NEAR)
-    return full.reshape(n, 5, cut).transpose(1, 0, 2).reshape(5, width), gathered
+    return full.reshape(n, 5, cut).transpose(1, 0, 2).reshape(5, width), gathered, held
 
 
 def modulated_norm(rows, norm_gain, shift_row, scale_row):
@@ -224,7 +225,9 @@
     high = lax.ppermute(jnp.concatenate([latent[:PAD], context[:PAD]]), SP, down)
     own = jnp.concatenate([latent, low[:PAD], high[:PAD]])
     context_rows = jnp.concatenate([low[PAD:], context, high[PAD:]])
-    mods, gathered = mod_vectors(cond, context_cond, modulation, own)
+    held = (conv_x, conv_b, conv_c, decay_rate, decay_extra, norm_gain, w_dt, out_gain)
+    mods, gathered, held = mod_vectors(cond, context_cond, modulation, own, held)
+    conv_x, conv_b, conv_c, decay_rate, decay_extra, norm_gain, w_dt, out_gain = held
     tokens_own = latent.shape[0]
     latent_rows = jnp.concatenate(
         [

time: 181 us -> 183 us (1.011)
  the two profiles are of different devices: /device:TPU:2 before, /device:TPU:6 now
where the time goes in v5:
time: 183 us; the launch traced here: 182 us
  waiting for transfers between devices  80.5 us (44%)
  starting transfers between devices  70.4 us (38%)
  matrix products  8.86 us (5%)
  blocking collectives  7.99 us (4%)
  local copies, waits for them, and re-layouts  7.31 us (4%)
  other arithmetic  4.19 us (2%)
  Pallas kernels  2.27 us (1%)
    all_to_all x6, waiting for transfers between devices, exchange(): return lax.all_to_all(x, axis, 0, 0, tiled=True)  72.8 us
    all_to_all x6, starting transfers between devices, exchange(): return lax.all_to_all(x, axis, 0, 0, tiled=True)  53.9 us
    ppermute x3, starting transfers between devices, ring_rows(): lax.ppermute(x, 'tp', [(i, (i + k) % n) for i in range(n)])  10.7 us
    all_to_all x1, blocking collectives, program(): lax.all_to_all(stacked, 'tp', split_axis=0, concat_axis=2, tiled=True)[0]  7.99 us
    ppermute x3, waiting for transfers between devices, ring_rows(): lax.ppermute(x, 'tp', [(i, (i + k) % n) for i in range(n)])  6.66 us
    ppermute x1, starting transfers between devices, program(): low = lax.ppermute(jnp.concatenate([latent[-PAD:], context[-PAD:]]), SP, up)  4.56 us
    dot_general x1, matrix products, program(): branch = jnp.dot(full, w_out, preferred_element_type=F32)  3.68 us
  transfers between devices with their start and end apart: 11, of which 9 were waited for; matrix products, arithmetic and copies ran while one was open for 2% of the time, Pallas kernels for 0%

profile of v5, /device:TPU:6, one launch (start us, length us, event | category | flops | bytes accessed | tf_op | source)
XLA Modules:
  0.0 182.4 jit_solution(9665870734558507295)
XLA Ops:
  0.0 2.3 %partial_mods.1 = f32[40,2,128]{2,1,0:T(2,128)} custom-call(s32[1]{0:T(128)} %bitcast.first, bf16[2048]{0:T(1024)(128)(2,1)} %cond.1, bf16[2048]{0:T(1024)(128)(2,1)} %context_cond.1, bf16[16,6144]{1,0:T(8,128)(2,1)} %modulation.1), custom_call_target="tpu_custom_call" | custom-call | tf_op jit(solution)/shard_map/partial_mods/pallas_call | solution.py:77
  2.3 5.8 %all-to-all-start = ((f32[40,2,128]{2,1,0:T(2,128)}), f32[40,2,128]{2,1,0:T(2,128)S(1)}, u32[]{:S(2)}, u32[]{:S(2)}) async-start(f32[40,2,128]{2,1,0:T(2,128)} %partial_mods.1), calls=%async_computation | async-start | bytes 81920 | tf_op jit(solution)/shard_map/all_to_all | solution.py:27
  8.1 0.8 fusion.141
  9.0 1.3 collective-permute-start.1
  10.3 4.6 %collective-permute-start = (bf16[16,2048]{1,0:T(8,128)(2,1)S(1)}, bf16[16,2048]{1,0:T(8,128)(2,1)S(1)}, u32[]{:S(2)}, u32[]{:S(2)}) collective-permute-start(bf16[16,2048]{1,0:T(8,128)(2,1)S(1)} %pad_maximum_fusion.11), channel_id=1, source_target_pairs={{0,32},{32,64},{64,96},{96,128},{128,160},{160,192},{192,224},{224... | collective-permute-start | bytes 196616 | tf_op jit(solution)/shard_map/ppermute | solution.py:224
  15.6 1.1 collective-permute-done
  16.8 5.1 %collective-permute-start.4 = (bf16[48,2048]{1,0:T(8,128)(2,1)S(1)}, bf16[48,2048]{1,0:T(8,128)(2,1)S(1)}, u32[]{:S(2)}, u32[]{:S(2)}) collective-permute-start(bf16[48,2048]{1,0:T(8,128)(2,1)S(1)} %get-tuple-element.42), channel_id=1, source_target_pairs={{0,24},{8,0},{16,8},{24,16},{1,25},{9,1},{17,9},{25,17},{2,26},{10... | collective-permute-start | bytes 589832 | tf_op jit(solution)/shard_map/ppermute | solution.py:38
  21.9 2.8 %collective-permute-start.3 = (bf16[48,2048]{1,0:T(8,128)(2,1)S(1)}, bf16[48,2048]{1,0:T(8,128)(2,1)S(1)}, u32[]{:S(2)}, u32[]{:S(2)}) collective-permute-start(bf16[48,2048]{1,0:T(8,128)(2,1)S(1)} %get-tuple-element.42), channel_id=1, source_target_pairs={{0,16},{8,24},{16,0},{24,8},{1,17},{9,25},{17,1},{25,9},{2,18},{10... | collective-permute-start | bytes 589832 | tf_op jit(solution)/shard_map/ppermute | solution.py:38
  24.7 2.8 %collective-permute-start.2 = (bf16[48,2048]{1,0:T(8,128)(2,1)S(1)}, bf16[48,2048]{1,0:T(8,128)(2,1)S(1)}, u32[]{:S(2)}, u32[]{:S(2)}) collective-permute-start(bf16[48,2048]{1,0:T(8,128)(2,1)S(1)} %get-tuple-element.42), channel_id=1, source_target_pairs={{0,8},{8,16},{16,24},{24,0},{1,9},{9,17},{17,25},{25,1},{2,10},{10... | collective-permute-start | bytes 589832 | tf_op jit(solution)/shard_map/ppermute | solution.py:38
  27.6 1.7 collective-permute-done.4
  29.3 2.9 %collective-permute-done.3 = bf16[48,2048]{1,0:T(8,128)(2,1)S(1)} collective-permute-done((bf16[48,2048]{1,0:T(8,128)(2,1)S(1)}, bf16[48,2048]{1,0:T(8,128)(2,1)S(1)}, u32[]{:S(2)}, u32[]{:S(2)}) %collective-permute-start.3) | collective-permute-done | bytes 196640 | tf_op jit(solution)/shard_map/ppermute | solution.py:38
  32.2 2.1 %collective-permute-done.2 = bf16[48,2048]{1,0:T(8,128)(2,1)S(1)} collective-permute-done((bf16[48,2048]{1,0:T(8,128)(2,1)S(1)}, bf16[48,2048]{1,0:T(8,128)(2,1)S(1)}, u32[]{:S(2)}, u32[]{:S(2)}) %collective-permute-start.2) | collective-permute-done | bytes 196640 | tf_op jit(solution)/shard_map/ppermute | solution.py:38
  34.6 0.2 fusion.2
  34.9 0.7 broadcast_in_dim.439
  35.5 29.4 %all-to-all-start.1 = ((f32[80,2,128]{2,1,0:T(2,128)}), f32[80,2,128]{2,1,0:T(2,128)S(1)}, u32[]{:S(2)}, u32[]{:S(2)}) async-start(f32[80,2,128]{2,1,0:T(2,128)} %bitcast.2), calls=%async_computation.1 | async-start | bytes 163840 | tf_op jit(solution)/shard_map/all_to_all | solution.py:27
  64.9 22.6 %all-to-all-done.1 = f32[80,2,128]{2,1,0:T(2,128)S(1)} async-done(((f32[80,2,128]{2,1,0:T(2,128)}), f32[80,2,128]{2,1,0:T(2,128)S(1)}, u32[]{:S(2)}, u32[]{:S(2)}) %all-to-all-start.1) | async-done | bytes 81952 | tf_op jit(solution)/shard_map/all_to_all | solution.py:27
  87.5 0.6 broadcast_in_dim.440
  88.2 3.4 %all-to-all-start.2 = ((f32[40,2,128]{2,1,0:T(2,128)}), f32[40,2,128]{2,1,0:T(2,128)S(1)}, u32[]{:S(2)}, u32[]{:S(2)}) async-start(f32[40,2,128]{2,1,0:T(2,128)} %bitcast.4), calls=%async_computation.2 | async-start | bytes 81920 | tf_op jit(solution)/shard_map/all_to_all | solution.py:27
  91.7 6.1 %all-to-all-done.2 = f32[40,2,128]{2,1,0:T(2,128)S(1)} async-done(((f32[40,2,128]{2,1,0:T(2,128)}), f32[40,2,128]{2,1,0:T(2,128)S(1)}, u32[]{:S(2)}, u32[]{:S(2)}) %all-to-all-start.2) | async-done | bytes 40992 | tf_op jit(solution)/shard_map/all_to_all | solution.py:27
  97.9 0.3 fusion.6
  98.3 0.3 compare_select_fusion
  98.7 0.2 fusion.138
  99.0 0.2 fusion.41
  99.1 0.2 fusion.139
  99.6 0.4 fusion.11
  100.1 0.4 fusion.8
  101.4 0.2 fusion.13
  102.0 0.2 fusion.12
  102.8 1.9 %concatenate.67 = bf16[8,72,128]{2,1,0:T(8,128)(2,1)} concatenate(bf16[8,32,128]{2,1,0:T(8,128)(2,1)S(1)} %bitcast.211, bf16[8,32,128]{2,1,0:T(8,128)(2,1)S(1)} %bitcast.212, bf16[8,1,128]{2,1,0:T(2,128)(2,1)S(1)} %copy.209, bf16[8,1,128]{2,1,0:T(2,128)(2,1)S(1)} %copy.210, bf16[8,1,128]{2,1,0:T(2,128)(2,1)S(1)} %copy.211, bf16[8,1,128]{2,1,0:T(2,128)(2,1)S(1)} %copy.212, ...), dimensions={1} | concatenate | bytes 294912 | tf_op jit(solution)/shard_map/concatenate | solution.py:173
  104.7 4.0 %all-to-all-start.3 = ((bf16[8,72,128]{2,1,0:T(8,128)(2,1)}), bf16[8,72,128]{2,1,0:T(8,128)(2,1)S(1)}, u32[]{:S(2)}, u32[]{:S(2)}) async-start(bf16[8,72,128]{2,1,0:T(8,128)(2,1)} %concatenate.67), calls=%async_computation.3 | async-start | bytes 294912 | tf_op jit(solution)/shard_map/all_to_all | solution.py:27
  108.7 0.3 fusion.15
  109.1 0.2 fusion.147
  109.3 0.2 fusion.48
  109.5 10.8 %all-to-all-done.3 = bf16[8,72,128]{2,1,0:T(8,128)(2,1)S(1)} async-done(((bf16[8,72,128]{2,1,0:T(8,128)(2,1)}), bf16[8,72,128]{2,1,0:T(8,128)(2,1)S(1)}, u32[]{:S(2)}, u32[]{:S(2)}) %all-to-all-start.3) | async-done | bytes 147488 | tf_op jit(solution)/shard_map/all_to_all | solution.py:27
  120.4 0.3 fusion.18
  121.1 0.6 broadcast_in_dim.480
  121.8 8.0 %all-to-all-start.4 = ((bf16[4,72,128]{2,1,0:T(8,128)(2,1)}), bf16[4,72,128]{2,1,0:T(8,128)(2,1)S(1)}, u32[]{:S(2)}, u32[]{:S(2)}) async-start(bf16[4,72,128]{2,1,0:T(8,128)(2,1)} %broadcast_in_dim.480), calls=%async_computation.4 | async-start | bytes 147456 | tf_op jit(solution)/shard_map/all_to_all | solution.py:27
  129.8 0.2 fusion.50
  130.0 23.1 %all-to-all-done.4 = bf16[4,72,128]{2,1,0:T(8,128)(2,1)S(1)} async-done(((bf16[4,72,128]{2,1,0:T(8,128)(2,1)}), bf16[4,72,128]{2,1,0:T(8,128)(2,1)S(1)}, u32[]{:S(2)}, u32[]{:S(2)}) %all-to-all-start.4) | async-done | bytes 73760 | tf_op jit(solution)/shard_map/all_to_all | solution.py:27
  153.7 0.6 fusion.25
  154.3 3.4 %all-to-all-start.5 = ((bf16[8,32,128]{2,1,0:T(8,128)(2,1)}), bf16[8,32,128]{2,1,0:T(8,128)(2,1)S(1)}, u32[]{:S(2)}, u32[]{:S(2)}) async-start(bf16[8,32,128]{2,1,0:T(8,128)(2,1)} %fusion.25), calls=%async_computation.5 | async-start | bytes 131072 | tf_op jit(solution)/shard_map/all_to_all | solution.py:27
  157.9 0.2 fusion.52
  158.1 0.2 fusion.54
  158.3 10.2 %all-to-all-done.5 = bf16[8,32,128]{2,1,0:T(8,128)(2,1)S(1)} async-done(((bf16[8,32,128]{2,1,0:T(8,128)(2,1)}), bf16[8,32,128]{2,1,0:T(8,128)(2,1)S(1)}, u32[]{:S(2)}, u32[]{:S(2)}) %all-to-all-start.5) | async-done | bytes 65568 | tf_op jit(solution)/shard_map/all_to_all | solution.py:27
  168.5 0.2 convolution_multiply_fusion.1
  168.9 1.6 multiply_reduce_fusion.4
  170.7 8.0 %all_to_all.46 = bf16[4,32,256]{2,1,0:T(8,128)(2,1)S(1)} all-to-all(bf16[4,32,256]{2,1,0:T(8,128)(2,1)S(1)} %bitcast.214), channel_id=1, replica_groups=mesh['za'=4,'zb'=4,'zc'=2,'tp'=4,'dp'=8] {'tp'}, dimensions={0} | all-to-all | bytes 131072 | tf_op jit(solution)/shard_map/all_to_all | solution.py:308
  178.8 3.7 %fusion.1 = bf16[32,2048]{1,0:T(8,128)(2,1)} fusion(bf16[32,1024]{1,0:T(8,128)(2,1)S(1)} %bitcast.210, bf16[1024,2048]{1,0:T(8,128)(2,1)} %param.35, bf16[32,2048]{1,0:T(8,128)(2,1)S(1)} %copy-done.1, f32[2048]{0:T(1024)S(1)} %bitcast.227), kind=kOutput, calls=%fused_computation.2 | convolution fusion | flops 134479872 | bytes 4530176 | tf_op jit(solution)/shard_map/dot_general | solution.py:309
  (143 shorter events, 5.4 us)
Async XLA Ops:
  0.0 100.1 %copy-start = (bf16[2048,256]{1,0:T(8,128)(2,1)S(1)}, bf16[2048,256]{1,0:T(8,128)(2,1)}, u32[]{:S(2)}) copy-start(bf16[2048,256]{1,0:T(8,128)(2,1)} %param.24) | copy-start | bytes 3145732
  0.0 16.7 %copy-start.1 = (bf16[32,2048]{1,0:T(8,128)(2,1)S(1)}, bf16[32,2048]{1,0:T(8,128)(2,1)}, u32[]{:S(2)}) copy-start(bf16[32,2048]{1,0:T(8,128)(2,1)} %param.18) | copy-start | bytes 393220
  0.0 27.5 %copy-start.2 = (bf16[16,2048]{1,0:T(8,128)(2,1)S(1)}, bf16[16,2048]{1,0:T(8,128)(2,1)}, u32[]{:S(2)}) copy-start(bf16[16,2048]{1,0:T(8,128)(2,1)} %param.20) | copy-start | bytes 196612
  2.3 32.5 %all-to-all-start = ((f32[40,2,128]{2,1,0:T(2,128)}), f32[40,2,128]{2,1,0:T(2,128)S(1)}, u32[]{:S(2)}, u32[]{:S(2)}) async-start(f32[40,2,128]{2,1,0:T(2,128)} %partial_mods.1), calls=%async_computation | async-start | bytes 81920 | tf_op jit(solution)/shard_map/all_to_all | solution.py:27
  9.0 6.7 %collective-permute-start.1 = (bf16[16,2048]{1,0:T(8,128)(2,1)S(1)}, bf16[16,2048]{1,0:T(8,128)(2,1)S(1)}, u32[]{:S(2)}, u32[]{:S(2)}) collective-permute-start(bf16[16,2048]{1,0:T(8,128)(2,1)S(1)} %pad_maximum_fusion.12), channel_id=1, source_target_pairs={{32,0},{64,32},{96,64},{128,96},{160,128},{192,160},{224,192},{256... | collective-permute-start | bytes 196616 | tf_op jit(solution)/shard_map/ppermute | solution.py:225
  10.3 6.5 %collective-permute-start = (bf16[16,2048]{1,0:T(8,128)(2,1)S(1)}, bf16[16,2048]{1,0:T(8,128)(2,1)S(1)}, u32[]{:S(2)}, u32[]{:S(2)}) collective-permute-start(bf16[16,2048]{1,0:T(8,128)(2,1)S(1)} %pad_maximum_fusion.11), channel_id=1, source_target_pairs={{0,32},{32,64},{64,96},{96,128},{128,160},{160,192},{192,224},{224... | collective-permute-start | bytes 196616 | tf_op jit(solution)/shard_map/ppermute | solution.py:224
  16.8 12.5 %collective-permute-start.4 = (bf16[48,2048]{1,0:T(8,128)(2,1)S(1)}, bf16[48,2048]{1,0:T(8,128)(2,1)S(1)}, u32[]{:S(2)}, u32[]{:S(2)}) collective-permute-start(bf16[48,2048]{1,0:T(8,128)(2,1)S(1)} %get-tuple-element.42), channel_id=1, source_target_pairs={{0,24},{8,0},{16,8},{24,16},{1,25},{9,1},{17,9},{25,17},{2,26},{10... | collective-permute-start | bytes 589832 | tf_op jit(solution)/shard_map/ppermute | solution.py:38
  21.9 10.3 %collective-permute-start.3 = (bf16[48,2048]{1,0:T(8,128)(2,1)S(1)}, bf16[48,2048]{1,0:T(8,128)(2,1)S(1)}, u32[]{:S(2)}, u32[]{:S(2)}) collective-permute-start(bf16[48,2048]{1,0:T(8,128)(2,1)S(1)} %get-tuple-element.42), channel_id=1, source_target_pairs={{0,16},{8,24},{16,0},{24,8},{1,17},{9,25},{17,1},{25,9},{2,18},{10... | collective-permute-start | bytes 589832 | tf_op jit(solution)/shard_map/ppermute | solution.py:38
  24.7 9.6 %collective-permute-start.2 = (bf16[48,2048]{1,0:T(8,128)(2,1)S(1)}, bf16[48,2048]{1,0:T(8,128)(2,1)S(1)}, u32[]{:S(2)}, u32[]{:S(2)}) collective-permute-start(bf16[48,2048]{1,0:T(8,128)(2,1)S(1)} %get-tuple-element.42), channel_id=1, source_target_pairs={{0,8},{8,16},{16,24},{24,0},{1,9},{9,17},{17,25},{25,1},{2,10},{10... | collective-permute-start | bytes 589832 | tf_op jit(solution)/shard_map/ppermute | solution.py:38
  34.5 30.4 %copy-start.4 = (bf16[2,2048,4]{1,2,0:T(4,128)(2,1)S(1)}, bf16[2,2048,4]{1,2,0:T(4,128)(2,1)}, u32[]{:S(2)}) copy-start(bf16[2,2048,4]{1,2,0:T(4,128)(2,1)} %param.28) | copy-start | bytes 98308
  34.5 57.0 %copy-start.5 = (bf16[4,256]{1,0:T(4,128)(2,1)S(1)}, bf16[4,256]{1,0:T(4,128)(2,1)}, u32[]{:S(2)}) copy-start(bf16[4,256]{1,0:T(4,128)(2,1)} %param.29) | copy-start | bytes 6148
  34.5 57.0 %copy-start.6 = (bf16[2048]{0:T(1024)(128)(2,1)S(1)}, bf16[2048]{0:T(1024)(128)(2,1)}, u32[]{:S(2)}) copy-start(bf16[2048]{0:T(1024)(128)(2,1)} %param.23) | copy-start | bytes 12292
  34.5 57.1 %copy-start.10 = (f32[2,4]{1,0:T(2,128)S(1)}, f32[2,4]{1,0:T(2,128)}, u32[]{:S(2)}) copy-start(f32[2,4]{1,0:T(2,128)} %param.32) | copy-start | bytes 100
  34.5 57.1 %copy-start.12 = (bf16[256]{0:T(256)(128)(2,1)S(1)}, bf16[256]{0:T(256)(128)(2,1)}, u32[]{:S(2)}) copy-start(bf16[256]{0:T(256)(128)(2,1)} %param.34) | copy-start | bytes 1540
  34.5 57.1 %copy-start.7 = (bf16[4,64]{1,0:T(4,128)(2,1)S(1)}, bf16[4,64]{1,0:T(4,128)(2,1)}, u32[]{:S(2)}) copy-start(bf16[4,64]{1,0:T(4,128)(2,1)} %param.31) | copy-start | bytes 1540
  34.6 57.1 %copy-start.8 = (bf16[4,64]{1,0:T(4,128)(2,1)S(1)}, bf16[4,64]{1,0:T(4,128)(2,1)}, u32[]{:S(2)}) copy-start(bf16[4,64]{1,0:T(4,128)(2,1)} %param.30) | copy-start | bytes 1540
  35.5 52.0 %all-to-all-start.1 = ((f32[80,2,128]{2,1,0:T(2,128)}), f32[80,2,128]{2,1,0:T(2,128)S(1)}, u32[]{:S(2)}, u32[]{:S(2)}) async-start(f32[80,2,128]{2,1,0:T(2,128)} %bitcast.2), calls=%async_computation.1 | async-start | bytes 163840 | tf_op jit(solution)/shard_map/all_to_all | solution.py:27
  88.2 9.7 %all-to-all-start.2 = ((f32[40,2,128]{2,1,0:T(2,128)}), f32[40,2,128]{2,1,0:T(2,128)S(1)}, u32[]{:S(2)}, u32[]{:S(2)}) async-start(f32[40,2,128]{2,1,0:T(2,128)} %bitcast.4), calls=%async_computation.2 | async-start | bytes 81920 | tf_op jit(solution)/shard_map/all_to_all | solution.py:27
  97.9 0.8 copy-start.9
  97.9 1.7 copy-start.11
  100.6 8.1 %copy-start.3 = (bf16[2048,64]{0,1:T(8,128)(2,1)S(1)}, bf16[2048,64]{0,1:T(8,128)(2,1)}, u32[]{:S(2)}) copy-start(bf16[2048,64]{0,1:T(8,128)(2,1)} %param.27) | copy-start | bytes 786436
  104.7 15.6 %all-to-all-start.3 = ((bf16[8,72,128]{2,1,0:T(8,128)(2,1)}), bf16[8,72,128]{2,1,0:T(8,128)(2,1)S(1)}, u32[]{:S(2)}, u32[]{:S(2)}) async-start(bf16[8,72,128]{2,1,0:T(8,128)(2,1)} %concatenate.67), calls=%async_computation.3 | async-start | bytes 294912 | tf_op jit(solution)/shard_map/all_to_all | solution.py:27
  121.8 31.3 %all-to-all-start.4 = ((bf16[4,72,128]{2,1,0:T(8,128)(2,1)}), bf16[4,72,128]{2,1,0:T(8,128)(2,1)S(1)}, u32[]{:S(2)}, u32[]{:S(2)}) async-start(bf16[4,72,128]{2,1,0:T(8,128)(2,1)} %broadcast_in_dim.480), calls=%async_computation.4 | async-start | bytes 147456 | tf_op jit(solution)/shard_map/all_to_all | solution.py:27
  154.3 14.2 %all-to-all-start.5 = ((bf16[8,32,128]{2,1,0:T(8,128)(2,1)}), bf16[8,32,128]{2,1,0:T(8,128)(2,1)S(1)}, u32[]{:S(2)}, u32[]{:S(2)}) async-start(bf16[8,32,128]{2,1,0:T(8,128)(2,1)} %fusion.25), calls=%async_computation.5 | async-start | bytes 131072 | tf_op jit(solution)/shard_map/all_to_all | solution.py:27
